TPU v7x, 32 devices: a whole 2x2x4 slice. The times are simulated.
32 devices in a mesh: sp: 16 (over z, y, x), tp: 2 (over core).
Axes of the slice: x: 2, y: 2, z: 4, core: 2. Of those that a mesh axis runs over, the one named last changes fastest.
Arguments:
- tokens: bfloat16 [6144, 2048], P('sp', 'tp'), may hold values from -6 to 6
- input_gain: float32 [2048], replicated, may hold values from 0.1 to 1.9
- query_weight: bfloat16 [2048, 1024], P(None, 'tp'), may hold values from -0.5 to 0.5
- query_rot_weight: bfloat16 [2048, 512], P(None, 'tp'), may hold values from -0.125 to 0.125
- kv_down: bfloat16 [2048, 256], replicated, may hold values from -0.5 to 0.5
- rot_down: bfloat16 [2048, 32], replicated, may hold values from -0.125 to 0.125
- kv_gain: float32 [256], replicated, may hold values from 0.1 to 1.9
- key_up: bfloat16 [256, 1024], P(None, 'tp'), may hold values from -0.5 to 0.5
- value_up: bfloat16 [256, 1024], P(None, 'tp'), may hold values from -4 to 4
- conv_value_weight: bfloat16 [2048, 1024], P(None, 'tp'), may hold values from -0.125 to 0.125
- conv_gate_weight: bfloat16 [2048, 1024], P(None, 'tp'), may hold values from -0.125 to 0.125
- conv_taps: float32 [31, 1024], P(None, 'tp'), may hold values from -8 to 8
- conv_ln_gain: float32 [1024], P('tp'), may hold values from 0.1 to 1.9
- conv_ln_bias: float32 [1024], P('tp'), may hold values from -3 to 3
- att_out_gain: float32 [1024], P('tp'), may hold values from 0.1 to 1.9
- conv_out_gain: float32 [1024], P('tp'), may hold values from 0.1 to 1.9
- att_out_weight: bfloat16 [1024, 2048], P('tp'), may hold values from -0.125 to 0.125
- conv_out_weight: bfloat16 [1024, 2048], P('tp'), may hold values from -0.125 to 0.125
Outputs:
- mixed: bfloat16 [6144, 2048], P('sp', 'tp')
All inputs are finite; a program needn't handle non-finite values.
Results may differ from a plain program's by a relative error of at most 0.017.
Values may be sent and summed in bfloat16 or wider, within the bound.
A program may use at most 128 MiB of HBM per device.

v0:
```python
import math

import jax
import jax.numpy as jnp
from jax import lax
from jax.sharding import PartitionSpec as P

D_MODEL = 2048
NOPE_DIM = 64
ROT_DIM = 32
VALUE_DIM = 64
CONV_CH = 1024
KERNEL = 31
ATT_WIDTH = 1024


norm_eps = 1e-06
far_below = -1e30
rope_base = 10000.0


def shifted(block, axis, distance):
    devices = range(lax.axis_size(axis))
    route = [(i - distance, i) for i in devices if i - distance in devices]
    return lax.ppermute(block, axis, route)


def rotary_tables(positions, half_dim):
    frequency = rope_base ** (-jnp.arange(half_dim, dtype=jnp.float32) / half_dim)
    angles = positions.astype(jnp.float32)[:, None] * frequency[None, :]
    return (jnp.cos(angles), jnp.sin(angles))


def rotate_half(values, cos_table, sine_table):
    half_dim = cos_table.shape[-1]
    front_half = values[..., :half_dim]
    back_half = values[..., half_dim:]
    return jnp.concatenate(
        [
            front_half * cos_table - back_half * sine_table,
            back_half * cos_table + front_half * sine_table,
        ],
        axis=-1,
    )


def shards(
    tokens,
    input_gain,
    query_weight,
    query_rot_weight,
    kv_down,
    rot_down,
    kv_gain,
    key_up,
    value_up,
    conv_value_weight,
    conv_gate_weight,
    conv_taps,
    conv_ln_gain,
    conv_ln_bias,
    att_out_gain,
    conv_out_gain,
    att_out_weight,
    conv_out_weight,
):
    tok_rows = tokens.shape[0]
    heads_here = key_up.shape[1] // NOPE_DIM
    chan_here = conv_taps.shape[1]
    weight_list = (
        query_weight,
        query_rot_weight,
        kv_down,
        rot_down,
        conv_value_weight,
        conv_gate_weight,
    )
    wide_part = lax.all_gather(tokens, "tp", axis=1, tiled=True).astype(jnp.float32)
    scaled = (wide_part * input_gain[None, :]).astype(jnp.bfloat16)

    def add_product(weight):
        return jnp.dot(scaled, weight, preferred_element_type=jnp.float32)

    summed = tuple((add_product(weight) for weight in weight_list))
    q_acc, qrot_acc, latent_raw, rot_acc, value_acc, gate_acc, square_sum = summed + (
        jnp.sum(wide_part * wide_part, axis=1),
    )
    row_scale = lax.rsqrt(square_sum / D_MODEL + norm_eps)[:, None]
    positions = lax.axis_index("sp") * tok_rows + jnp.arange(tok_rows, dtype=jnp.int32)
    cos_table, sine_table = rotary_tables(positions, ROT_DIM // 2)
    queries = (q_acc * row_scale).astype(jnp.bfloat16).reshape(tok_rows, heads_here, NOPE_DIM)
    query_rot = rotate_half(
        (qrot_acc * row_scale).reshape(tok_rows, heads_here, ROT_DIM),
        cos_table[:, None, :],
        sine_table[:, None, :],
    ).astype(jnp.bfloat16)
    latent = (
        latent_raw
        * lax.rsqrt(jnp.mean(latent_raw * latent_raw, axis=1, keepdims=True) + norm_eps)
        * kv_gain[None, :]
    ).astype(jnp.bfloat16)
    key_rot = rotate_half(rot_acc * row_scale, cos_table, sine_table).astype(jnp.bfloat16)
    gated_input = (value_acc * row_scale * jax.nn.sigmoid(gate_acc * row_scale)).astype(
        jnp.bfloat16
    )
    query_end = (lax.axis_index("sp") + 1) * tok_rows
    inv_scale = 1.0 / math.sqrt(NOPE_DIM + ROT_DIM)

    def attend(carried, key_block, rot_block, value_block, key_offset):
        run_max, run_sum, run_acc = carried
        block_len = key_block.shape[0]
        scores = (
            jnp.einsum("qhd,khd->hqk", queries, key_block, preferred_element_type=jnp.float32)
            + jnp.einsum("qhd,kd->hqk", query_rot, rot_block, preferred_element_type=jnp.float32)
        ) * inv_scale
        key_pos = key_offset + jnp.arange(block_len, dtype=jnp.int32)
        visible = (key_pos[None, :] <= positions[:, None])[None]
        new_max = jnp.maximum(run_max, jnp.max(jnp.where(visible, scores, far_below), axis=2))
        exp_scores = jnp.where(visible, jnp.exp(scores - new_max[:, :, None]), 0.0)
        shrink = jnp.exp(run_max - new_max)
        run_sum = run_sum * shrink + jnp.sum(exp_scores, axis=2)
        run_acc = run_acc * shrink.T[:, :, None] + jnp.einsum(
            "hqk,khd->qhd",
            exp_scores.astype(jnp.bfloat16),
            value_block,
            preferred_element_type=jnp.float32,
        )
        return (new_max, run_sum, run_acc)

    def expand_latent(sliced):
        lat_block, rot_block = sliced
        key_block = (
            jnp.dot(lat_block, key_up, preferred_element_type=jnp.float32)
            .astype(jnp.bfloat16)
            .reshape(-1, heads_here, NOPE_DIM)
        )
        value_block = (
            jnp.dot(lat_block, value_up, preferred_element_type=jnp.float32)
            .astype(jnp.bfloat16)
            .reshape(-1, heads_here, VALUE_DIM)
        )
        return (key_block, value_block, rot_block)

    def square_rows(matrix):
        wide_rows = matrix.astype(jnp.float32)
        return jnp.sum(wide_rows * wide_rows, axis=1)

    start_state = (
        jnp.full((heads_here, tok_rows), far_below, jnp.float32),
        jnp.zeros((heads_here, tok_rows), jnp.float32),
        jnp.zeros((tok_rows, heads_here, VALUE_DIM), jnp.float32),
    )
    pieces = (
        lax.all_gather(latent, "sp", axis=0, tiled=True),
        lax.all_gather(key_rot, "sp", axis=0, tiled=True),
    )
    piece_rows = pieces[0].shape[0]
    step_len = math.gcd(piece_rows, 512)

    def visit_block(running, block_idx):
        start_row = block_idx * step_len
        sliced = tuple(
            (lax.dynamic_slice_in_dim(member, start_row, step_len, 0) for member in pieces)
        )

        def compute(current):
            key_block, value_block, rot_block = expand_latent(sliced)
            return attend(current, key_block, rot_block, value_block, start_row)

        return (lax.cond(start_row < query_end, compute, lambda current: current, running), None)

    final_state = lax.scan(
        visit_block, start_state, jnp.arange(piece_rows // step_len, dtype=jnp.int32)
    )[0]
    run_max, run_sum, run_acc = final_state
    attended = (
        (run_acc / run_sum.T[:, :, None])
        .astype(jnp.bfloat16)
        .reshape(tok_rows, heads_here * VALUE_DIM)
    )
    att_sq = lax.psum(square_rows(attended), "tp")
    rim_rows = shifted(gated_input[tok_rows - (KERNEL - 1) :], "sp", 1)
    padded = jnp.concatenate([rim_rows, gated_input], axis=0)
    conv_out = jnp.zeros((tok_rows, chan_here), jnp.float32)
    for tap_idx in range(KERNEL):
        conv_out = conv_out + conv_taps[tap_idx][None, :] * padded[
            tap_idx : tap_idx + tok_rows
        ].astype(jnp.float32)
    moment_one, moment_two = lax.psum(
        (jnp.sum(conv_out, axis=1), jnp.sum(conv_out * conv_out, axis=1)), "tp"
    )
    mean_val = moment_one / CONV_CH
    spread = moment_two / CONV_CH - mean_val * mean_val
    normed = (conv_out - mean_val[:, None]) * lax.rsqrt(spread + norm_eps)[:, None]
    swished = jax.nn.silu(normed * conv_ln_gain[None, :] + conv_ln_bias[None, :])
    conv_sq = lax.psum(square_rows(swished), "tp")
    att_mixed = (
        attended.astype(jnp.float32)
        * lax.rsqrt(att_sq / ATT_WIDTH + norm_eps)[:, None]
        * att_out_gain[None, :]
    ).astype(jnp.bfloat16)
    conv_mixed = (
        swished * lax.rsqrt(conv_sq / CONV_CH + norm_eps)[:, None] * conv_out_gain[None, :]
    ).astype(jnp.bfloat16)
    contract = (((0,), (1,)), ((), ()))
    feature_rows = lax.psum_scatter(
        (
            lax.dot_general(att_out_weight, att_mixed, contract, preferred_element_type=jnp.float32)
            + lax.dot_general(
                conv_out_weight, conv_mixed, contract, preferred_element_type=jnp.float32
            )
        ).astype(jnp.bfloat16),
        "tp",
        scatter_dimension=0,
        tiled=True,
    ).astype(jnp.float32)
    return feature_rows.T.astype(jnp.bfloat16)


def solution(mesh):
    return jax.shard_map(
        shards,
        mesh=mesh,
        in_specs=(
            P("sp", "tp"),
            P(),
            P(None, "tp"),
            P(None, "tp"),
            P(),
            P(),
            P(),
            P(None, "tp"),
            P(None, "tp"),
            P(None, "tp"),
            P(None, "tp"),
            P(None, "tp"),
            P("tp"),
            P("tp"),
            P("tp"),
            P("tp"),
            P("tp", None),
            P("tp", None),
        ),
        out_specs=P("sp", "tp"),
        check_vma=False,
    )
```

profile of v0, /device:TPU:31, one launch (start us, length us, event | category | flops | bytes accessed | tf_op | source)
XLA Modules:
  0.0 247.3 jit_solution(14839390345446647439)
XLA Ops:
  7.3 13.0 %all-gather.3.cloned.1.call-done = bf16[384,2048]{1,0:T(8,128)(2,1)} async-done(((bf16[384,1024]{1,0:T(8,128)(2,1)}), bf16[384,2048]{1,0:T(8,128)(2,1)}) %all-gather.3.cloned.1.call-update) | async-done | bytes 1572880 | tf_op jit(solution)/shard_map/all_gather | solution.py:78
  20.3 2.5 %multiply_reduce_fusion.3 = (f32[384]{0:T(512)S(1)}, f32[384,256]{0,1:T(8,128)S(1)}) fusion(bf16[2048,256]{1,0:T(8,128)(2,1)} %param.26, bf16[384,2048]{1,0:T(8,128)(2,1)} %all-gather.3.cloned.1.call-done, f32[2048]{0:T(1024)} %param.23), kind=kOutput, calls=%fused_computation.128 | convolution fusion | flops 405208704 | bytes 3024384 | tf_op jit(solution)/shard_map/dot_general | solution.py:82
  24.5 1.8 fusion.27
  26.3 3.3 %fusion.33 = f32[384,512]{1,0:T(8,128)S(1)} fusion(bf16[2048,512]{1,0:T(8,128)(2,1)} %param.32, bf16[384,2048]{1,0:T(8,128)(2,1)} %all-gather.3.cloned.1.call-done, f32[2048]{0:T(1024)S(1)} %copy-done.16, f32[384]{0:T(512)S(1)} %add_rsqrt_fusion.3), kind=kOutput, calls=%fused_computation.72 | convolution fusion | flops 808452096 | bytes 4466176 | tf_op jit(solution)/shard_map/dot_general | solution.py:82
  30.7 1.4 collective-permute-start
  32.9 33.7 %all_gather.11 = bf16[6144,32]{0,1:T(8,128)(2,1)} all-gather(bf16[384,32]{0,1:T(8,128)(2,1)S(1)} %pad_maximum_fusion.2), channel_id=1, replica_groups=mesh['sp'=16,'tp'=2] {'sp'}, dimensions={0}, use_global_device_ids=true | all-gather | bytes 417792 | tf_op jit(solution)/shard_map/all_gather | solution.py:155
  68.7 14.7 %fusion.77 = (f32[384]{0:T(512)}, f32[384]{0:T(512)}, f32[384,512]{1,0:T(8,128)S(1)}) fusion(bf16[384,512]{1,0:T(8,128)(2,1)} %copy-done.5, f32[512]{0:T(512)S(1)} %bitcast.93, bf16[30,512]{1,0:T(8,128)(2,1)S(1)} %collective-permute-done, f32[512]{0:T(512)S(1)} %bitcast.94, f32[512]{0:T(512)} %bitcast.96, f32[512]{0:T(512)} %bitcast.97, f32[512]{0:T(512)} %bitcast.98, ...), kind=kLoop, calls=%fused_computation.145 | loop fusion | flops 36371712 | bytes 1276928 | tf_op jit(solution)/shard_map/reduce_sum | solution.py:190
  83.4 9.8 %all-reduce.1 = (f32[384]{0:T(512)S(1)}, f32[384]{0:T(512)S(1)}) all-reduce(f32[384]{0:T(512)} %get-tuple-element.271, f32[384]{0:T(512)} %get-tuple-element.270), channel_id=1, replica_groups=mesh['sp'=16,'tp'=2] {'tp'}, use_global_device_ids=true, to_apply=%region_13.14 | all-reduce | flops 768 | bytes 6144 | tf_op jit(solution)/shard_map/psum | solution.py:189
  94.4 4.7 %copy.24 = bf16[6144,256]{1,0:T(8,128)(2,1)} copy(bf16[6144,256]{0,1:T(8,128)(2,1)} %all-gather.5.cloned.1.call-done) | data formatting | bytes 6291456
  99.1 122.8 %while.15 = (s32[]{:T(128)}, f32[8,384]{1,0:T(8,128)S(1)}, f32[8,384]{1,0:T(8,128)S(1)}, f32[384,8,64]{0,2,1:T(8,128)S(1)}, s32[12]{0:T(128)S(1)}, /*index=5*/s3...) while((s32[]{:T(128)}, f32[8,384]{1,0:T(8,128)S(1)}, ...), condition=%wide.region_7.8_spmd.clone, body=%wide.region_2.7_spmd.clone.sunk | while | flops 788604800 | bytes 38840728 | solution.py:172
  100.4 9.0 %conditional.3 = ((f32[8,384]{1,0:T(8,128)S(1)}, f32[8,384]{1,0:T(8,128)S(1)}, f32[384,8,64]{0,2,1:T(8,128)S(1)})) conditional(s32[]{:T(128)} %convert_element_type.326, (f32[8,384]{1,0:T(8,128)S(1)}, f32[8,384]{1,0:T(8,128)S(1)}, f32[384,8,64]{0,2,1:T(8,128)S(1)}) %tuple.85, (s32[]{:T(128)}, s32[]{:T(128)}, bf16[6144,256]{1,0:T(8,128)(2,1)}, ...), branch_computations={%region_3.3_spmd, %region_4.6_spmd} | conditional | flops 788604800 | bytes 38838896 | solution.py:170
  100.4 1.4 convolution_convert_fusion.1
  101.8 1.9 fusion.18
  103.9 1.6 select_reduce_fusion
  106.8 1.4 fusion.13
  110.6 9.0 %conditional.3 = ((f32[8,384]{1,0:T(8,128)S(1)}, f32[8,384]{1,0:T(8,128)S(1)}, f32[384,8,64]{0,2,1:T(8,128)S(1)})) conditional(s32[]{:T(128)} %convert_element_type.326, (f32[8,384]{1,0:T(8,128)S(1)}, f32[8,384]{1,0:T(8,128)S(1)}, f32[384,8,64]{0,2,1:T(8,128)S(1)}) %tuple.85, (s32[]{:T(128)}, s32[]{:T(128)}, bf16[6144,256]{1,0:T(8,128)(2,1)}, ...), branch_computations={%region_3.3_spmd, %region_4.6_spmd} | conditional | flops 788604800 | bytes 38838896 | solution.py:170
  110.6 1.4 convolution_convert_fusion.1
  112.0 1.9 fusion.18
  114.1 1.6 select_reduce_fusion
  117.0 1.4 fusion.13
  120.9 9.0 %conditional.3 = ((f32[8,384]{1,0:T(8,128)S(1)}, f32[8,384]{1,0:T(8,128)S(1)}, f32[384,8,64]{0,2,1:T(8,128)S(1)})) conditional(s32[]{:T(128)} %convert_element_type.326, (f32[8,384]{1,0:T(8,128)S(1)}, f32[8,384]{1,0:T(8,128)S(1)}, f32[384,8,64]{0,2,1:T(8,128)S(1)}) %tuple.85, (s32[]{:T(128)}, s32[]{:T(128)}, bf16[6144,256]{1,0:T(8,128)(2,1)}, ...), branch_computations={%region_3.3_spmd, %region_4.6_spmd} | conditional | flops 788604800 | bytes 38838896 | solution.py:170
  122.3 1.9 fusion.18
  124.3 1.6 select_reduce_fusion
  127.3 1.4 fusion.13
  131.1 9.0 %conditional.3 = ((f32[8,384]{1,0:T(8,128)S(1)}, f32[8,384]{1,0:T(8,128)S(1)}, f32[384,8,64]{0,2,1:T(8,128)S(1)})) conditional(s32[]{:T(128)} %convert_element_type.326, (f32[8,384]{1,0:T(8,128)S(1)}, f32[8,384]{1,0:T(8,128)S(1)}, f32[384,8,64]{0,2,1:T(8,128)S(1)}) %tuple.85, (s32[]{:T(128)}, s32[]{:T(128)}, bf16[6144,256]{1,0:T(8,128)(2,1)}, ...), branch_computations={%region_3.3_spmd, %region_4.6_spmd} | conditional | flops 788604800 | bytes 38838896 | solution.py:170
  132.5 1.9 fusion.18
  134.6 1.6 select_reduce_fusion
  137.5 1.4 fusion.13
  141.3 9.0 %conditional.3 = ((f32[8,384]{1,0:T(8,128)S(1)}, f32[8,384]{1,0:T(8,128)S(1)}, f32[384,8,64]{0,2,1:T(8,128)S(1)})) conditional(s32[]{:T(128)} %convert_element_type.326, (f32[8,384]{1,0:T(8,128)S(1)}, f32[8,384]{1,0:T(8,128)S(1)}, f32[384,8,64]{0,2,1:T(8,128)S(1)}) %tuple.85, (s32[]{:T(128)}, s32[]{:T(128)}, bf16[6144,256]{1,0:T(8,128)(2,1)}, ...), branch_computations={%region_3.3_spmd, %region_4.6_spmd} | conditional | flops 788604800 | bytes 38838896 | solution.py:170
  142.7 1.9 fusion.18
  144.8 1.6 select_reduce_fusion
  147.7 1.4 fusion.13
  151.5 9.0 %conditional.3 = ((f32[8,384]{1,0:T(8,128)S(1)}, f32[8,384]{1,0:T(8,128)S(1)}, f32[384,8,64]{0,2,1:T(8,128)S(1)})) conditional(s32[]{:T(128)} %convert_element_type.326, (f32[8,384]{1,0:T(8,128)S(1)}, f32[8,384]{1,0:T(8,128)S(1)}, f32[384,8,64]{0,2,1:T(8,128)S(1)}) %tuple.85, (s32[]{:T(128)}, s32[]{:T(128)}, bf16[6144,256]{1,0:T(8,128)(2,1)}, ...), branch_computations={%region_3.3_spmd, %region_4.6_spmd} | conditional | flops 788604800 | bytes 38838896 | solution.py:170
  153.0 1.9 fusion.18
  155.0 1.6 select_reduce_fusion
  158.0 1.4 fusion.13
  161.8 9.0 %conditional.3 = ((f32[8,384]{1,0:T(8,128)S(1)}, f32[8,384]{1,0:T(8,128)S(1)}, f32[384,8,64]{0,2,1:T(8,128)S(1)})) conditional(s32[]{:T(128)} %convert_element_type.326, (f32[8,384]{1,0:T(8,128)S(1)}, f32[8,384]{1,0:T(8,128)S(1)}, f32[384,8,64]{0,2,1:T(8,128)S(1)}) %tuple.85, (s32[]{:T(128)}, s32[]{:T(128)}, bf16[6144,256]{1,0:T(8,128)(2,1)}, ...), branch_computations={%region_3.3_spmd, %region_4.6_spmd} | conditional | flops 788604800 | bytes 38838896 | solution.py:170
  163.2 1.9 fusion.18
  165.3 1.6 select_reduce_fusion
  168.2 1.4 fusion.13
  172.0 9.0 %conditional.3 = ((f32[8,384]{1,0:T(8,128)S(1)}, f32[8,384]{1,0:T(8,128)S(1)}, f32[384,8,64]{0,2,1:T(8,128)S(1)})) conditional(s32[]{:T(128)} %convert_element_type.326, (f32[8,384]{1,0:T(8,128)S(1)}, f32[8,384]{1,0:T(8,128)S(1)}, f32[384,8,64]{0,2,1:T(8,128)S(1)}) %tuple.85, (s32[]{:T(128)}, s32[]{:T(128)}, bf16[6144,256]{1,0:T(8,128)(2,1)}, ...), branch_computations={%region_3.3_spmd, %region_4.6_spmd} | conditional | flops 788604800 | bytes 38838896 | solution.py:170
  173.4 1.9 fusion.18
  175.5 1.6 select_reduce_fusion
  178.4 1.4 fusion.13
  182.2 9.0 %conditional.3 = ((f32[8,384]{1,0:T(8,128)S(1)}, f32[8,384]{1,0:T(8,128)S(1)}, f32[384,8,64]{0,2,1:T(8,128)S(1)})) conditional(s32[]{:T(128)} %convert_element_type.326, (f32[8,384]{1,0:T(8,128)S(1)}, f32[8,384]{1,0:T(8,128)S(1)}, f32[384,8,64]{0,2,1:T(8,128)S(1)}) %tuple.85, (s32[]{:T(128)}, s32[]{:T(128)}, bf16[6144,256]{1,0:T(8,128)(2,1)}, ...), branch_computations={%region_3.3_spmd, %region_4.6_spmd} | conditional | flops 788604800 | bytes 38838896 | solution.py:170
  183.7 1.9 fusion.18
  185.7 1.6 select_reduce_fusion
  188.7 1.4 fusion.13
  192.5 9.0 %conditional.3 = ((f32[8,384]{1,0:T(8,128)S(1)}, f32[8,384]{1,0:T(8,128)S(1)}, f32[384,8,64]{0,2,1:T(8,128)S(1)})) conditional(s32[]{:T(128)} %convert_element_type.326, (f32[8,384]{1,0:T(8,128)S(1)}, f32[8,384]{1,0:T(8,128)S(1)}, f32[384,8,64]{0,2,1:T(8,128)S(1)}) %tuple.85, (s32[]{:T(128)}, s32[]{:T(128)}, bf16[6144,256]{1,0:T(8,128)(2,1)}, ...), branch_computations={%region_3.3_spmd, %region_4.6_spmd} | conditional | flops 788604800 | bytes 38838896 | solution.py:170
  193.9 1.9 fusion.18
  196.0 1.6 select_reduce_fusion
  198.9 1.4 fusion.13
  202.7 9.0 %conditional.3 = ((f32[8,384]{1,0:T(8,128)S(1)}, f32[8,384]{1,0:T(8,128)S(1)}, f32[384,8,64]{0,2,1:T(8,128)S(1)})) conditional(s32[]{:T(128)} %convert_element_type.326, (f32[8,384]{1,0:T(8,128)S(1)}, f32[8,384]{1,0:T(8,128)S(1)}, f32[384,8,64]{0,2,1:T(8,128)S(1)}) %tuple.85, (s32[]{:T(128)}, s32[]{:T(128)}, bf16[6144,256]{1,0:T(8,128)(2,1)}, ...), branch_computations={%region_3.3_spmd, %region_4.6_spmd} | conditional | flops 788604800 | bytes 38838896 | solution.py:170
  204.1 1.9 fusion.18
  206.2 1.6 select_reduce_fusion
  209.1 1.4 fusion.13
  212.9 8.9 %conditional.3 = ((f32[8,384]{1,0:T(8,128)S(1)}, f32[8,384]{1,0:T(8,128)S(1)}, f32[384,8,64]{0,2,1:T(8,128)S(1)})) conditional(s32[]{:T(128)} %convert_element_type.326, (f32[8,384]{1,0:T(8,128)S(1)}, f32[8,384]{1,0:T(8,128)S(1)}, f32[384,8,64]{0,2,1:T(8,128)S(1)}) %tuple.85, (s32[]{:T(128)}, s32[]{:T(128)}, bf16[6144,256]{1,0:T(8,128)(2,1)}, ...), branch_computations={%region_3.3_spmd, %region_4.6_spmd} | conditional | flops 788604800 | bytes 38838896 | solution.py:170
  214.3 1.8 fusion.18
  216.4 1.6 select_reduce_fusion
  219.3 1.4 fusion.13
  222.9 2.5 all-reduce
  225.4 1.4 fusion.37
  227.9 2.5 fusion.28
  230.4 10.4 %reduce-scatter.2.cloned.1.call-done = bf16[1024,384]{0,1:T(8,128)(2,1)} async-done(((bf16[2048,384]{0,1:T(8,128)(2,1)}), bf16[1024,384]{0,1:T(8,128)(2,1)}) %reduce-scatter.2.cloned.1.call-update) | async-done | bytes 786448 | tf_op jit(solution)/shard_map/reduce_scatter | solution.py:206
  (222 shorter events, 61.5 us)
Async XLA Ops:
  6.5 220.3 %copy-start = (bf16[512,2048]{1,0:T(8,128)(2,1)S(1)}, bf16[512,2048]{1,0:T(8,128)(2,1)}, u32[]{:S(2)}) copy-start(bf16[512,2048]{1,0:T(8,128)(2,1)} %param.38) | copy-start | bytes 6291460
  6.5 16.3 %copy-start.10 = (f32[256]{0:T(256)S(1)}, f32[256]{0:T(256)}, u32[]{:S(2)}) copy-start(f32[256]{0:T(256)} %param.28) | copy-start | bytes 3076
  6.5 17.2 %copy-start.6 = (f32[31,512]{1,0:T(8,128)S(1)}, f32[31,512]{1,0:T(8,128)}, u32[]{:S(2)}) copy-start(f32[31,512]{1,0:T(8,128)} %param.33) | copy-start | bytes 190468
  6.5 13.8 %all-gather.3.cloned.1.call-start = ((), (), s32[]{:S(2)}) async-start(), calls=%async_computation.1 | async-start | bytes 2359296 | tf_op jit(solution)/shard_map/all_gather | solution.py:78
  7.3 19.0 %copy-start.16 = (f32[2048]{0:T(1024)S(1)}, f32[2048]{0:T(1024)}, u32[]{:S(2)}) copy-start(f32[2048]{0:T(1024)} %param.23) | copy-start | bytes 24580
  7.3 87.1 %all-gather.5.cloned.1.call-start = ((), (), s32[]{:S(2)}) async-start(), calls=%async_computation.2 | async-start | bytes 3342336 | tf_op jit(solution)/shard_map/all_gather | solution.py:154
  23.7 217.1 %reduce-scatter.2.cloned.1.call-start = ((), (), s32[]{:S(2)}) async-start(), calls=%async_computation.3 | async-start | bytes 2359296 | tf_op jit(solution)/shard_map/reduce_scatter | solution.py:206
  26.3 3.4 %copy-start.4 = (bf16[384,2048]{1,0:T(8,128)(2,1)S(1)}, bf16[384,2048]{1,0:T(8,128)(2,1)}, u32[]{:S(2)}) copy-start(bf16[384,2048]{1,0:T(8,128)(2,1)} %all-gather.3.cloned.1.call-done) | copy-start | bytes 4718596
  26.3 3.4 %copy-start.11 = (bf16[2048,512]{1,0:T(8,128)(2,1)S(1)}, bf16[2048,512]{1,0:T(8,128)(2,1)}, u32[]{:S(2)}) copy-start(bf16[2048,512]{1,0:T(8,128)(2,1)} %param.31) | copy-start | bytes 6291460
  29.6 2.5 %copy-start.15 = (bf16[2048,32]{0,1:T(8,128)(2,1)S(1)}, bf16[2048,32]{0,1:T(8,128)(2,1)}, u32[]{:S(2)}) copy-start(bf16[2048,32]{0,1:T(8,128)(2,1)} %param.27) | copy-start | bytes 393220
  29.7 37.0 %copy-start.14 = (bf16[2048,256]{1,0:T(8,128)(2,1)S(1)}, bf16[2048,256]{1,0:T(8,128)(2,1)}, u32[]{:S(2)}) copy-start(bf16[2048,256]{1,0:T(8,128)(2,1)} %param.25) | copy-start | bytes 3145732
  30.7 36.8 %copy-start.5 = (bf16[384,512]{1,0:T(8,128)(2,1)}, bf16[384,512]{1,0:T(8,128)(2,1)S(1)}, u32[]{:S(2)}) copy-start(bf16[384,512]{1,0:T(8,128)(2,1)S(1)} %fusion.35) | copy-start | bytes 1179652
  30.7 36.8 %copy-start.12 = (bf16[2048,512]{1,0:T(8,128)(2,1)S(1)}, bf16[2048,512]{1,0:T(8,128)(2,1)}, u32[]{:S(2)}) copy-start(bf16[2048,512]{1,0:T(8,128)(2,1)} %param.24) | copy-start | bytes 6291460
  30.7 38.0 %collective-permute-start = (bf16[30,512]{1,0:T(8,128)(2,1)S(1)}, bf16[30,512]{1,0:T(8,128)(2,1)S(1)}, u32[]{:S(2)}, u32[]{:S(2)}) collective-permute-start(bf16[30,512]{1,0:T(8,128)(2,1)S(1)} %slice.268), channel_id=1, source_target_pairs={{0,2},{2,4},{4,6},{6,8},{8,10},{10,12},{12,14},{14,16},{16,18},{18... | collective-permute-start | bytes 92168 | tf_op jit(solution)/shard_map/ppermute | solution.py:25
  83.4 15.6 %copy-start.2 = (f32[384,512]{1,0:T(8,128)}, f32[384,512]{1,0:T(8,128)S(1)}, u32[]{:S(2)}) copy-start(f32[384,512]{1,0:T(8,128)S(1)} %get-tuple-element.304) | copy-start | bytes 2359300
  99.1 126.2 %copy-start.7 = (f32[512]{0:T(512)S(1)}, f32[512]{0:T(512)}, u32[]{:S(2)}) copy-start(f32[512]{0:T(512)} %param.36) | copy-start | bytes 6148
  103.9 1.6 copy-start.1
  114.1 1.6 copy-start.1
  124.3 1.6 copy-start.1
  134.6 1.6 copy-start.1
  144.8 1.6 copy-start.1
  155.0 1.6 copy-start.1
  165.3 1.6 copy-start.1
  175.5 1.6 copy-start.1
  185.7 1.6 copy-start.1
  196.0 1.6 copy-start.1
  206.2 1.6 copy-start.1
  216.4 1.6 copy-start.1
  225.3 2.5 %copy-start.3 = (f32[384,512]{1,0:T(8,128)S(1)}, f32[384,512]{1,0:T(8,128)}, u32[]{:S(2)}) copy-start(f32[384,512]{1,0:T(8,128)} %copy-done.2) | copy-start | bytes 2359300
  225.3 2.5 %copy-start.8 = (f32[512]{0:T(512)S(1)}, f32[512]{0:T(512)}, u32[]{:S(2)}) copy-start(f32[512]{0:T(512)} %param.35) | copy-start | bytes 6148
  225.3 2.5 %copy-start.9 = (f32[512]{0:T(512)S(1)}, f32[512]{0:T(512)}, u32[]{:S(2)}) copy-start(f32[512]{0:T(512)} %param.34) | copy-start | bytes 6148
  225.4 2.5 %copy-start.13 = (bf16[512,2048]{1,0:T(8,128)(2,1)S(1)}, bf16[512,2048]{1,0:T(8,128)(2,1)}, u32[]{:S(2)}) copy-start(bf16[512,2048]{1,0:T(8,128)(2,1)} %param.39) | copy-start | bytes 6291460
  225.4 2.5 %copy-start.17 = (f32[512]{0:T(512)S(1)}, f32[512]{0:T(512)}, u32[]{:S(2)}) copy-start(f32[512]{0:T(512)} %param.37) | copy-start | bytes 6148
Sparse Core Ops, SparseCore 0:
  8.9 11.4 all-gather.2
  23.8 68.3 all-gather.4
  230.5 10.2 reduce-scatter.1
where the time goes:
time: 250 us; the launch traced here: 247 us
  matrix products  103 us (41%)
  blocking collectives  45.9 us (18%)
  other arithmetic  36.6 us (15%)
  waiting for transfers between devices  24.2 us (10%)
  between operations  13.5 us (5%)
  local copies, waits for them, and re-layouts  12.9 us (5%)
  loops' own time  9.66 us (4%)
    all_gather x1, blocking collectives, shards(): lax.all_gather(key_rot, 'sp', axis=0, tiled=True)  33.7 us
    dot_general x12, matrix products, attend(): jnp.einsum('qhd,kd->hqk', query_rot, rot_block, preferred_element_type=jn...  22.3 us
    dot_general x12, matrix products, attend(): jnp.einsum('qhd,khd->hqk', queries, key_block, preferred_element_type=jnp...  19.1 us
    dot_general x12, matrix products, attend(): jnp.einsum('hqk,khd->qhd', exp_scores.astype(jnp.bfloat16), value_block,...  16.9 us
    dot_general x12, matrix products, expand_latent(): jnp.dot(lat_block, key_up, preferred_element_type=jnp.float32)  16.6 us
    dot_general x12, matrix products, expand_latent(): jnp.dot(lat_block, value_up, preferred_element_type=jnp.float32)  15.6 us
    reduce_sum x1, other arithmetic, shards(): jnp.sum(conv_out, axis=1)  14.7 us
    reduce_sum x12, other arithmetic, attend(): run_sum = run_sum * shrink + jnp.sum(exp_scores, axis=2)  13.1 us
  transfers between devices with their start and end apart: 4, of which 2 were waited for; matrix products, arithmetic and copies ran while one was open for 10% of the time, Pallas kernels for 0%

commit v1 on v0

v1 whole, which is shorter than its diff:
```python
import math

import jax
import jax.numpy as jnp
from jax import lax
from jax.experimental import pallas as pl
from jax.experimental.pallas import tpu as pltpu
from jax.sharding import PartitionSpec as P

D_MODEL = 2048
NOPE_DIM = 64
ROT_DIM = 32
VALUE_DIM = 64
CONV_CH = 1024
KERNEL = 31
ATT_WIDTH = 1024


norm_eps = 1e-06
far_below = -1e30
rope_base = 10000.0


def shifted(block, axis, distance):
    devices = range(lax.axis_size(axis))
    route = [(i - distance, i) for i in devices if i - distance in devices]
    return lax.ppermute(block, axis, route)


def rotary_tables(positions, half_dim):
    frequency = rope_base ** (-jnp.arange(half_dim, dtype=jnp.float32) / half_dim)
    angles = positions.astype(jnp.float32)[:, None] * frequency[None, :]
    return (jnp.cos(angles), jnp.sin(angles))


def rotate_half(values, cos_table, sine_table):
    half_dim = cos_table.shape[-1]
    front_half = values[..., :half_dim]
    back_half = values[..., half_dim:]
    return jnp.concatenate(
        [
            front_half * cos_table - back_half * sine_table,
            back_half * cos_table + front_half * sine_table,
        ],
        axis=-1,
    )


def attention_kernel(q_ref, lat_ref, kup_ref, vup_ref, o_ref, kt, vt, run_max, acc):
    heads, rows, lanes = q_ref.shape
    blocks = lat_ref.shape[0]
    rank = kup_ref.shape[1]
    nope = kup_ref.shape[0] // heads
    vdim = vup_ref.shape[0] // heads
    rot = lat_ref.shape[1] - rank
    wide = kt.shape[2]
    group = wide // rows
    me = lax.axis_index("sp")
    last = me // group
    kt[:, nope + rot :, :] = jnp.zeros((heads, lanes - nope - rot, wide), jnp.bfloat16)
    vt[:, vdim:, :] = jnp.ones((heads, lanes - vdim, wide), jnp.bfloat16)

    def expand(block):
        for part in range(group):
            src = jnp.minimum(block * group + part, blocks - 1)
            lat = lat_ref[src, :rank, :]
            turned = lat_ref[src, rank:, :]
            cols = slice(part * rows, (part + 1) * rows)
            keys = jnp.dot(kup_ref[...], lat, preferred_element_type=jnp.float32)
            values = jnp.dot(vup_ref[...], lat, preferred_element_type=jnp.float32)
            for head in range(heads):
                kt[head, :nope, cols] = keys[head * nope : (head + 1) * nope].astype(jnp.bfloat16)
                kt[head, nope : nope + rot, cols] = turned
                vt[head, :vdim, cols] = values[head * vdim : (head + 1) * vdim].astype(
                    jnp.bfloat16
                )

    def weigh(head, scores, top):
        weights = jnp.exp2(scores - top).astype(jnp.bfloat16)
        return lax.dot_general(
            weights, vt[head], (((1,), (1,)), ((), ())), preferred_element_type=jnp.float32
        )

    expand(last)
    key_pos = last * wide + lax.broadcasted_iota(jnp.int32, (rows, wide), 1)
    query_pos = me * rows + lax.broadcasted_iota(jnp.int32, (rows, wide), 0)
    hidden = key_pos > query_pos
    for head in range(heads):
        scores = jnp.dot(q_ref[head], kt[head], preferred_element_type=jnp.float32)
        scores = jnp.where(hidden, far_below, scores)
        top = jnp.max(scores, axis=1, keepdims=True)
        run_max[head] = jnp.broadcast_to(top, (rows, lanes))
        acc[head] = weigh(head, scores, top)

    def visit(step, carry):
        expand(step)
        for head in range(heads):
            scores = jnp.dot(q_ref[head], kt[head], preferred_element_type=jnp.float32)
            old = run_max[head]
            top = jnp.maximum(old[:, :1], jnp.max(scores, axis=1, keepdims=True))
            wide_top = jnp.broadcast_to(top, (rows, lanes))
            run_max[head] = wide_top
            acc[head] = acc[head] * jnp.exp2(old - wide_top) + weigh(head, scores, top)
        return carry

    lax.fori_loop(0, last, visit, 0)
    lane = lax.broadcasted_iota(jnp.int32, (rows, lanes), 1)
    for pair in range(heads // 2):
        halves = []
        for head in (2 * pair, 2 * pair + 1):
            total = acc[head]
            halves.append(total / pltpu.roll(total, vdim, axis=1))
        both = jnp.where(lane < vdim, halves[0], pltpu.roll(halves[1], vdim, axis=1))
        o_ref[:, pair * lanes : (pair + 1) * lanes] = both.astype(jnp.bfloat16)


def attention(q_heads, lat_all, key_up_t, value_up_t):
    heads, rows, lanes = q_heads.shape
    blocks = lat_all.shape[0]
    wide = 2 * rows if blocks % 2 == 0 else rows
    vmem = pl.BlockSpec(memory_space=pltpu.VMEM)
    return pl.pallas_call(
        attention_kernel,
        out_shape=jax.ShapeDtypeStruct((rows, value_up_t.shape[0]), jnp.bfloat16),
        in_specs=[vmem] * 4,
        out_specs=vmem,
        scratch_shapes=[
            pltpu.VMEM((heads, lanes, wide), jnp.bfloat16),
            pltpu.VMEM((heads, lanes, wide), jnp.bfloat16),
            pltpu.VMEM((heads, rows, lanes), jnp.float32),
            pltpu.VMEM((heads, rows, lanes), jnp.float32),
        ],
        compiler_params=pltpu.CompilerParams(vmem_limit_bytes=48 << 20),
        cost_estimate=pl.CostEstimate(
            flops=20_000_000_000, bytes_accessed=8 << 20, transcendentals=20_000_000
        ),
        name="attention",
    )(q_heads, lat_all, key_up_t, value_up_t)


def conv_kernel(gated_ref, rim_ref, taps_ref, out_ref, wide):
    rows, chans = gated_ref.shape
    rim = rim_ref.shape[0]
    taps = taps_ref.shape[0]
    chunk = 64
    for part in range(chans // 128):
        cols = slice(part * 128, (part + 1) * 128)
        wide[part, :rim, :] = rim_ref[:, cols].astype(jnp.float32)
        wide[part, rim:, :] = gated_ref[:, cols].astype(jnp.float32)
        coeff = taps_ref[:, cols]

        def band(step, carry):
            base = step * chunk
            total = jnp.zeros((chunk, 128), jnp.float32)
            for tap in range(taps):
                total = total + coeff[tap : tap + 1, :] * wide[
                    part, pl.ds(base + (rim - taps + 1 + tap), chunk), :
                ]
            out_ref[pl.ds(pl.multiple_of(base, chunk), chunk), cols] = total
            return carry

        lax.fori_loop(0, rows // chunk, band, 0)


def convolve(gated, rim, taps):
    rows, chans = gated.shape
    vmem = pl.BlockSpec(memory_space=pltpu.VMEM)
    return pl.pallas_call(
        conv_kernel,
        out_shape=jax.ShapeDtypeStruct((rows, chans), jnp.float32),
        in_specs=[vmem] * 3,
        out_specs=vmem,
        scratch_shapes=[pltpu.VMEM((chans // 128, rows + rim.shape[0], 128), jnp.float32)],
        cost_estimate=pl.CostEstimate(
            flops=2 * rows * chans * 31, bytes_accessed=2 << 20, transcendentals=0
        ),
        name="depthwise",
    )(gated, rim, taps)


def shards(
    tokens,
    input_gain,
    query_weight,
    query_rot_weight,
    kv_down,
    rot_down,
    kv_gain,
    key_up,
    value_up,
    conv_value_weight,
    conv_gate_weight,
    conv_taps,
    conv_ln_gain,
    conv_ln_bias,
    att_out_gain,
    conv_out_gain,
    att_out_weight,
    conv_out_weight,
):
    tok_rows = tokens.shape[0]
    heads_here = key_up.shape[1] // NOPE_DIM
    chan_here = conv_taps.shape[1]
    weight_list = (
        query_weight,
        query_rot_weight,
        kv_down,
        rot_down,
        conv_value_weight,
        conv_gate_weight,
    )
    wide_part = lax.all_gather(tokens, "tp", axis=1, tiled=True).astype(jnp.float32)
    scaled = (wide_part * input_gain[None, :]).astype(jnp.bfloat16)

    def add_product(weight):
        return jnp.dot(scaled, weight, preferred_element_type=jnp.float32)

    summed = tuple((add_product(weight) for weight in weight_list))
    q_acc, qrot_acc, latent_raw, rot_acc, value_acc, gate_acc, square_sum = summed + (
        jnp.sum(wide_part * wide_part, axis=1),
    )
    row_scale = lax.rsqrt(square_sum / D_MODEL + norm_eps)[:, None]
    positions = lax.axis_index("sp") * tok_rows + jnp.arange(tok_rows, dtype=jnp.int32)
    cos_table, sine_table = rotary_tables(positions, ROT_DIM // 2)
    fold = math.log2(math.e) / math.sqrt(NOPE_DIM + ROT_DIM)
    query_scale = row_scale * fold
    plain_q = (q_acc * query_scale).reshape(tok_rows, heads_here, NOPE_DIM)
    turned_q = rotate_half(
        (qrot_acc * query_scale).reshape(tok_rows, heads_here, ROT_DIM),
        cos_table[:, None, :],
        sine_table[:, None, :],
    )
    blank = jnp.zeros((tok_rows, heads_here, 128 - NOPE_DIM - ROT_DIM), jnp.float32)
    q_heads = jnp.transpose(
        jnp.concatenate([plain_q, turned_q, blank], axis=2).astype(jnp.bfloat16), (1, 0, 2)
    )
    latent = (
        latent_raw
        * lax.rsqrt(jnp.mean(latent_raw * latent_raw, axis=1, keepdims=True) + norm_eps)
        * kv_gain[None, :]
    ).astype(jnp.bfloat16)
    key_rot = rotate_half(rot_acc * row_scale, cos_table, sine_table).astype(jnp.bfloat16)
    gated_input = (value_acc * row_scale * jax.nn.sigmoid(gate_acc * row_scale)).astype(
        jnp.bfloat16
    )
    def square_rows(matrix):
        wide_rows = matrix.astype(jnp.float32)
        return jnp.sum(wide_rows * wide_rows, axis=1)

    packed = jnp.concatenate([latent.T, key_rot.T], axis=0)
    lat_all = lax.all_gather(packed, "sp", axis=0)
    rim_rows = shifted(gated_input[tok_rows - (KERNEL + 1) :], "sp", 1)
    conv_out = convolve(gated_input, rim_rows, conv_taps)
    attended = attention(q_heads, lat_all, key_up.T, value_up.T)
    att_sq = lax.psum(square_rows(attended), "tp")
    moment_one, moment_two = lax.psum(
        (jnp.sum(conv_out, axis=1), jnp.sum(conv_out * conv_out, axis=1)), "tp"
    )
    mean_val = moment_one / CONV_CH
    spread = moment_two / CONV_CH - mean_val * mean_val
    normed = (conv_out - mean_val[:, None]) * lax.rsqrt(spread + norm_eps)[:, None]
    swished = jax.nn.silu(normed * conv_ln_gain[None, :] + conv_ln_bias[None, :])
    conv_sq = lax.psum(square_rows(swished), "tp")
    att_mixed = (
        attended.astype(jnp.float32)
        * lax.rsqrt(att_sq / ATT_WIDTH + norm_eps)[:, None]
        * att_out_gain[None, :]
    ).astype(jnp.bfloat16)
    conv_mixed = (
        swished * lax.rsqrt(conv_sq / CONV_CH + norm_eps)[:, None] * conv_out_gain[None, :]
    ).astype(jnp.bfloat16)
    contract = (((0,), (1,)), ((), ()))
    feature_rows = lax.psum_scatter(
        (
            lax.dot_general(att_out_weight, att_mixed, contract, preferred_element_type=jnp.float32)
            + lax.dot_general(
                conv_out_weight, conv_mixed, contract, preferred_element_type=jnp.float32
            )
        ).astype(jnp.bfloat16),
        "tp",
        scatter_dimension=0,
        tiled=True,
    ).astype(jnp.float32)
    return feature_rows.T.astype(jnp.bfloat16)


def solution(mesh):
    return jax.shard_map(
        shards,
        mesh=mesh,
        in_specs=(
            P("sp", "tp"),
            P(),
            P(None, "tp"),
            P(None, "tp"),
            P(),
            P(),
            P(),
            P(None, "tp"),
            P(None, "tp"),
            P(None, "tp"),
            P(None, "tp"),
            P(None, "tp"),
            P("tp"),
            P("tp"),
            P("tp"),
            P("tp"),
            P("tp", None),
            P("tp", None),
        ),
        out_specs=P("sp", "tp"),
        check_vma=False,
    )
```

time: 250 us -> 172 us (0.69)
  matrix products: 103 us -> 16 us
  Pallas kernels: 0 us -> 52.2 us
  blocking collectives: 45.9 us -> 7.12 us
  waiting for transfers between devices: 24.2 us -> 62.9 us
  other arithmetic: 36.6 us -> 7.24 us
  loops' own time: 9.66 us -> 0 us
  local copies, waits for them, and re-layouts: 12.9 us -> 9.93 us
    dot_general x60 -> x0, matrix products: 90.5 us -> none  [the longest x12 22.3 us: attend(): jnp.einsum('qhd,kd->hqk', query_rot, rot_block, preferred_element_type=jn...]
    pallas_call x0 -> x2, Pallas kernels: none -> 52.2 us  [the longest x1 48.1 us: attention(): pl.pallas_call(attention_kernel, out_shape=jax.ShapeDtypeStruct((rows, va...]
    all_gather x1, waiting for transfers between devices: 0.02 us -> 36.5 us  [shards(): lat_all = lax.all_gather(packed, 'sp', axis=0)]
    all_gather x1 -> x0, blocking collectives: 33.7 us -> none  [shards(): lax.all_gather(key_rot, 'sp', axis=0, tiled=True)]
    reduce_sum x1, other arithmetic: 14.7 us -> 1.31 us  [shards(): jnp.sum(conv_out, axis=1)]
    reduce_sum x12 -> x0, other arithmetic: 13.1 us -> none  [attend(): run_sum = run_sum * shrink + jnp.sum(exp_scores, axis=2)]
    another operation x13 -> x0, loops' own time: 9.66 us -> none  [the longest x1 8.29 us: shards(): lax.scan(visit_block, start_state, jnp.arange(piece_rows // step_len, dty...]
    dynamic_slice x12 -> x0, local copies, waits for them, and re-layouts: 7.04 us -> none  [shards(): lax.scan(visit_block, start_state, jnp.arange(piece_rows // step_len, dty...]
  transfers between devices with their start and end apart: 4 -> 4, of which waited for: 2 -> 4; matrix products, arithmetic and copies ran while one was open for 10% -> 12% of each run, Pallas kernels for 0% -> 2%
where the time goes in v1:
time: 172 us; the launch traced here: 170 us
  waiting for transfers between devices  62.9 us (37%)
  Pallas kernels  52.2 us (30%)
  matrix products  16 us (9%)
  between operations  13.5 us (8%)
  local copies, waits for them, and re-layouts  9.93 us (6%)
  other arithmetic  7.24 us (4%)
  blocking collectives  7.12 us (4%)
    pallas_call x1, Pallas kernels, attention(): pl.pallas_call(attention_kernel, out_shape=jax.ShapeDtypeStruct((rows, va...  48.1 us
    all_gather x1, waiting for transfers between devices, shards(): lat_all = lax.all_gather(packed, 'sp', axis=0)  36.5 us
    all_gather x1, waiting for transfers between devices, shards(): lax.all_gather(tokens, 'tp', axis=1, tiled=True).astype(jnp.float32)  13 us
    dot_general x6, matrix products, add_product(): return jnp.dot(scaled, weight, preferred_element_type=jnp.float32)  12.5 us
    reduce_scatter x1, waiting for transfers between devices, shards(): lax.psum_scatter((lax.dot_general(att_out_weight, att_mixed, contract, pr...  10.4 us
    unnamed x54, local copies, waits for them, and re-layouts  8.19 us
    pallas_call x1, Pallas kernels, convolve(): pl.pallas_call(conv_kernel, out_shape=jax.ShapeDtypeStruct((rows, chans),...  4.06 us
    psum x1, blocking collectives, shards(): lax.psum((jnp.sum(conv_out, axis=1), jnp.sum(conv_out * conv_out, axis=1)...  3.67 us
  transfers between devices with their start and end apart: 4, of which 4 were waited for; matrix products, arithmetic and copies ran while one was open for 12% of the time, Pallas kernels for 2%

profile of v1, /device:TPU:31, one launch (start us, length us, event | category | flops | bytes accessed | tf_op | source)
XLA Modules:
  0.0 170.3 jit_solution(422819892332178599)
XLA Ops:
  6.5 0.0 copy-start
  6.5 0.0 all-gather.4.cloned.1.call-start
  6.5 0.7 all-gather.4.cloned.1.call-update
  7.3 0.0 all-gather.6.cloned.1.call-start
  7.3 13.0 %all-gather.4.cloned.1.call-done = bf16[384,2048]{1,0:T(8,128)(2,1)} async-done(((bf16[384,1024]{1,0:T(8,128)(2,1)}), bf16[384,2048]{1,0:T(8,128)(2,1)}) %all-gather.4.cloned.1.call-update) | async-done | bytes 1572880 | tf_op jit(solution)/shard_map/all_gather | solution.py:212
  20.3 1.9 %fusion.1 = f32[384]{0:T(512)S(1)} fusion(bf16[384,2048]{1,0:T(8,128)(2,1)} %all-gather.4.cloned.1.call-done), kind=kLoop, calls=%fused_computation.3 | loop fusion | flops 2358912 | bytes 1574400 | tf_op jit(solution)/shard_map/reduce_sum | solution.py:220
  22.3 0.0 copy-start.20
  22.3 2.0 %multiply_reduce_fusion.2 = (f32[384]{0:T(512)S(1)}, f32[384,256]{0,1:T(8,128)S(1)}) fusion(bf16[2048,256]{1,0:T(8,128)(2,1)} %param.22, bf16[384,2048]{1,0:T(8,128)(2,1)S(1)} %copy-done.7, f32[2048]{0:T(1024)S(1)} %copy-done.21), kind=kOutput, calls=%fused_computation.37 | convolution fusion | flops 405208704 | bytes 3024384 | tf_op jit(solution)/shard_map/dot_general | solution.py:216
  24.3 0.0 copy-start.17
  24.4 0.0 copy-start.10
  24.4 0.0 copy-start.11
  24.4 0.6 convolution_multiply_fusion.4
  25.0 0.2 subtract_convert_fusion.1
  25.2 0.1 fusion.26
  25.3 0.7 pad_maximum_fusion
  26.0 0.0 all-gather.6.cloned.1.call-update
  26.0 0.0 reduce-scatter.2.cloned.1.call-start
  26.1 0.1 copy.29
  26.3 0.9 copy.30
  27.1 0.1 pad.7.clone
  27.2 2.5 %convolution_multiply_fusion.3 = f32[384,256]{0,1:T(8,128)S(1)} fusion(bf16[2048,256]{1,0:T(8,128)(2,1)} %param.21, bf16[384,2048]{1,0:T(8,128)(2,1)} %all-gather.4.cloned.1.call-done, f32[2048]{0:T(1024)S(1)} %copy-done.21, f32[384]{0:T(512)S(1)} %get-tuple-element.22), kind=kOutput, calls=%fused_computation.18 | convolution fusion | flops 405110784 | bytes 3024384 | tf_op jit(solution)/shard_map/dot_general | solution.py:216
  29.7 1.7 copy.32
  31.4 1.7 copy.31
  33.0 0.1 copy.27
  33.2 0.1 copy.25
  33.3 0.0 copy-done.22
  33.3 3.1 %fusion.8 = bf16[384,512]{1,0:T(8,128)(2,1)S(1)} fusion(bf16[2048,512]{1,0:T(8,128)(2,1)} %param.20, bf16[384,2048]{1,0:T(8,128)(2,1)} %all-gather.4.cloned.1.call-done, f32[2048]{0:T(1024)S(1)} %copy-done.22, f32[384]{0:T(512)S(1)} %get-tuple-element.22), kind=kOutput, calls=%fused_computation.16 | convolution fusion | flops 808058880 | bytes 4072960 | tf_op jit(solution)/shard_map/dot_general | solution.py:216
  36.4 0.2 copy.23
  36.6 1.2 copy.28
  37.8 3.3 %fusion.7 = f32[384,512]{1,0:T(8,128)S(1)} fusion(bf16[2048,512]{1,0:T(8,128)(2,1)} %param.28, bf16[384,2048]{1,0:T(8,128)(2,1)} %all-gather.4.cloned.1.call-done, f32[2048]{0:T(1024)} %param.19, f32[384]{0:T(512)S(1)} %get-tuple-element.21), kind=kOutput, calls=%fused_computation.15 | convolution fusion | flops 808452096 | bytes 4466176 | tf_op jit(solution)/shard_map/dot_general | solution.py:216
  41.2 1.0 fusion.9.gated_ref
  42.2 0.0 copy-start.9
  42.2 0.0 copy-start.6
  42.2 1.4 collective-permute-start
  43.7 0.4 subtract_convert_fusion
  44.1 0.0 copy-done.9
  44.2 0.0 copy-done.6
  44.2 0.8 maximum_bitcast_fusion.q_ref
  44.9 0.0 copy-start.13
  44.9 0.0 copy-start.15
  45.0 2.2 %collective-permute-done.rim_ref = bf16[32,512]{1,0:T(8,128)(2,1)} collective-permute-done((bf16[32,512]{1,0:T(8,128)(2,1)S(1)}, bf16[32,512]{1,0:T(8,128)(2,1)}, u32[]{:S(2)}, u32[]{:S(2)}) %collective-permute-start) | collective-permute-done | bytes 32800 | tf_op jit(solution)/shard_map/ppermute | solution.py:27
  47.1 4.1 %depthwise.1 = f32[384,512]{1,0:T(8,128)} custom-call(bf16[384,512]{1,0:T(8,128)(2,1)} %copy-done.9, bf16[32,512]{1,0:T(8,128)(2,1)} %collective-permute-done.rim_ref, f32[31,512]{1,0:T(8,128)} %taps_ref.1), custom_call_target="tpu_custom_call" | custom-call | flops 12189696 | bytes 2097152 | tf_op jit(solution)/shard_map/depthwise/pallas_call | solution.py:168
  51.2 1.3 fusion.27
  52.5 3.7 %all-reduce.1 = (f32[384]{0:T(512)S(1)}, f32[384]{0:T(512)S(1)}) all-reduce(f32[384]{0:T(512)S(1)} %get-tuple-element.6, f32[384]{0:T(512)S(1)} %get-tuple-element.5), channel_id=1, replica_groups=mesh['sp'=16,'tp'=2] {'tp'}, use_global_device_ids=true, to_apply=%region_7.0 | all-reduce | flops 768 | bytes 6144 | tf_op jit(solution)/shard_map/psum | solution.py:256
  56.2 1.6 multiply_reduce_fusion
  57.8 36.5 %all-gather.6.cloned.1.call-done = bf16[4608,384]{1,0:T(8,128)(2,1)} async-done(((bf16[288,384]{1,0:T(8,128)(2,1)}), bf16[4608,384]{1,0:T(8,128)(2,1)}) %all-gather.6.cloned.1.call-update) | async-done | bytes 3538960 | tf_op jit(solution)/shard_map/all_gather | solution.py:251
  94.3 0.9 copy-done.1
  95.3 2.0 %copy-done.2 = bf16[4608,384]{1,0:T(8,128)(2,1)S(1)} copy-done((bf16[4608,384]{1,0:T(8,128)(2,1)S(1)}, bf16[4608,384]{1,0:T(8,128)(2,1)}, u32[]{:S(2)}) %copy-start.2) | copy-done | bytes 3538968
  97.3 48.1 %attention.1 = bf16[384,512]{1,0:T(8,128)(2,1)S(1)} custom-call(bf16[8,384,128]{2,1,0:T(8,128)(2,1)S(1)} %maximum_bitcast_fusion.q_ref, bf16[16,288,384]{2,1,0:T(8,128)(2,1)S(1)} %bitcast.24, bf16[512,256]{1,0:T(8,128)(2,1)S(1)} %bitcast.22, bf16[512,256]{1,0:T(8,128)(2,1)S(1)} %bitcast.23), custom_call_target="tpu_custom_call" | custom-call | flops 20000000000 | bytes 8388608 | tf_op jit(solution)/shard_map/attention/pallas_call | solution.py:122
  145.4 0.2 fusion.10
  145.6 3.5 %all-reduce = (f32[384]{0:T(512)S(1)}, f32[384]{0:T(512)S(1)}) all-reduce(f32[384]{0:T(512)S(1)} %fusion.10, f32[384]{0:T(512)S(1)} %multiply_reduce_fusion), channel_id=1, replica_groups=mesh['sp'=16,'tp'=2] {'tp'}, use_global_device_ids=true, to_apply=%region_3.0 | all-reduce | flops 768 | bytes 6144 | tf_op jit(solution)/shard_map/psum | solution.py:255
  149.0 0.0 copy-done
  149.1 0.0 copy-start.3
  149.1 0.0 copy-start.14
  149.1 0.0 copy-start.16
  149.1 0.0 copy-start.19
  149.1 0.0 copy-start.24
  149.1 1.0 fusion.20
  150.2 0.0 copy-done.3
  150.2 0.0 copy-done.14
  150.2 0.7 copy-done.19
  150.9 2.4 %fusion.2 = bf16[2048,384]{0,1:T(8,128)(2,1)} fusion(f32[384,2048]{1,0:T(8,128)S(1)} %fusion.20, bf16[512,2048]{1,0:T(8,128)(2,1)S(1)} %copy-done.19, f32[512]{0:T(512)S(1)} %copy-done.24, f32[384]{0:T(512)S(1)} %get-tuple-element.25, f32[384,512]{1,0:T(8,128)S(1)} %copy-done.3, f32[512]{0:T(512)S(1)} %copy-done.14, f32[512]{0:T(512)S(1)} %copy-done.16, ...), kind=kOutput, calls=%fused_computation.5 | convolution fusion | flops 809041920 | bytes 7612928 | tf_op jit(solution)/shard_map/dot_general | solution.py:276
  153.4 0.0 reduce-scatter.2.cloned.1.call-update
  153.4 10.4 %reduce-scatter.2.cloned.1.call-done = bf16[1024,384]{0,1:T(8,128)(2,1)} async-done(((bf16[2048,384]{0,1:T(8,128)(2,1)}), bf16[1024,384]{0,1:T(8,128)(2,1)}) %reduce-scatter.2.cloned.1.call-update) | async-done | bytes 786448 | tf_op jit(solution)/shard_map/reduce_scatter | solution.py:273
  (37 shorter events, 0.1 us)
Async XLA Ops:
  6.5 142.5 %copy-start = (bf16[512,2048]{1,0:T(8,128)(2,1)S(1)}, bf16[512,2048]{1,0:T(8,128)(2,1)}, u32[]{:S(2)}) copy-start(bf16[512,2048]{1,0:T(8,128)(2,1)} %param.34) | copy-start | bytes 6291460
  6.5 15.7 %copy-start.21 = (f32[2048]{0:T(1024)S(1)}, f32[2048]{0:T(1024)}, u32[]{:S(2)}) copy-start(f32[2048]{0:T(1024)} %param.19) | copy-start | bytes 24580
  6.5 13.8 %all-gather.4.cloned.1.call-start = ((), (), s32[]{:S(2)}) async-start(), calls=%async_computation.1 | async-start | bytes 2359296 | tf_op jit(solution)/shard_map/all_gather | solution.py:212
  7.3 87.1 %all-gather.6.cloned.1.call-start = ((), (), s32[]{:S(2)}) async-start(), calls=%async_computation.3 | async-start | bytes 3760128 | tf_op jit(solution)/shard_map/all_gather | solution.py:251
  20.3 1.9 %copy-start.7 = (bf16[384,2048]{1,0:T(8,128)(2,1)S(1)}, bf16[384,2048]{1,0:T(8,128)(2,1)}, u32[]{:S(2)}) copy-start(bf16[384,2048]{1,0:T(8,128)(2,1)} %all-gather.4.cloned.1.call-done) | copy-start | bytes 4718596
  22.3 2.1 %copy-start.20 = (bf16[2048,32]{0,1:T(8,128)(2,1)S(1)}, bf16[2048,32]{0,1:T(8,128)(2,1)}, u32[]{:S(2)}) copy-start(bf16[2048,32]{0,1:T(8,128)(2,1)} %param.23) | copy-start | bytes 393220
  24.3 0.8 copy-start.17
  24.4 1.7 %copy-start.10 = (bf16[256,512]{1,0:T(8,128)(2,1)S(1)}, bf16[256,512]{1,0:T(8,128)(2,1)}, u32[]{:S(2)}) copy-start(bf16[256,512]{1,0:T(8,128)(2,1)} %param.25) | copy-start | bytes 786436
  24.4 1.9 %copy-start.11 = (bf16[256,512]{1,0:T(8,128)(2,1)S(1)}, bf16[256,512]{1,0:T(8,128)(2,1)}, u32[]{:S(2)}) copy-start(bf16[256,512]{1,0:T(8,128)(2,1)} %param.26) | copy-start | bytes 786436
  26.0 137.8 %reduce-scatter.2.cloned.1.call-start = ((), (), s32[]{:S(2)}) async-start(), calls=%async_computation.2 | async-start | bytes 2359296 | tf_op jit(solution)/shard_map/reduce_scatter | solution.py:273
  31.4 1.9 %copy-start.22 = (f32[2048]{0:T(1024)S(1)}, f32[2048]{0:T(1024)}, u32[]{:S(2)}) copy-start(f32[2048]{0:T(1024)} %param.19) | copy-start | bytes 24580
  37.8 3.4 %copy-start.8 = (bf16[384,2048]{1,0:T(8,128)(2,1)S(1)}, bf16[384,2048]{1,0:T(8,128)(2,1)}, u32[]{:S(2)}) copy-start(bf16[384,2048]{1,0:T(8,128)(2,1)} %all-gather.4.cloned.1.call-done) | copy-start | bytes 4718596
  37.8 3.4 %copy-start.18 = (bf16[2048,512]{1,0:T(8,128)(2,1)S(1)}, bf16[2048,512]{1,0:T(8,128)(2,1)}, u32[]{:S(2)}) copy-start(bf16[2048,512]{1,0:T(8,128)(2,1)} %param.27) | copy-start | bytes 6291460
  37.8 3.4 %copy-start.23 = (f32[2048]{0:T(1024)S(1)}, f32[2048]{0:T(1024)}, u32[]{:S(2)}) copy-start(f32[2048]{0:T(1024)} %param.19) | copy-start | bytes 24580
  41.2 2.5 %copy-start.4 = (f32[384,8,16]{2,0,1:T(8,128)S(1)}, f32[384,8,16]{2,0,1:T(8,128)}, u32[]{:S(2)}) copy-start(f32[384,8,16]{2,0,1:T(8,128)} %copy.32) | copy-start | bytes 589828
  41.2 2.5 %copy-start.5 = (f32[384,8,16]{2,0,1:T(8,128)S(1)}, f32[384,8,16]{2,0,1:T(8,128)}, u32[]{:S(2)}) copy-start(f32[384,8,16]{2,0,1:T(8,128)} %copy.31) | copy-start | bytes 589828
  42.2 1.9 %copy-start.9 = (bf16[384,512]{1,0:T(8,128)(2,1)}, bf16[384,512]{1,0:T(8,128)(2,1)S(1)}, u32[]{:S(2)}) copy-start(bf16[384,512]{1,0:T(8,128)(2,1)S(1)} %fusion.9.gated_ref) | copy-start | bytes 1179652
  42.2 1.9 %copy-start.6 = (bf16[384,8,64]{2,0,1:T(8,128)(2,1)S(1)}, bf16[384,8,64]{2,0,1:T(8,128)(2,1)}, u32[]{:S(2)}) copy-start(bf16[384,8,64]{2,0,1:T(8,128)(2,1)} %copy.28) | copy-start | bytes 1179652
  42.2 4.9 %collective-permute-start = (bf16[32,512]{1,0:T(8,128)(2,1)S(1)}, bf16[32,512]{1,0:T(8,128)(2,1)}, u32[]{:S(2)}, u32[]{:S(2)}) collective-permute-start(bf16[32,512]{1,0:T(8,128)(2,1)S(1)} %slice.24), channel_id=1, source_target_pairs={{0,2},{2,4},{4,6},{6,8},{8,10},{10,12},{12,14},{14,16},{16,18},{18... | collective-permute-start | bytes 98312 | tf_op jit(solution)/shard_map/ppermute | solution.py:27
  44.9 11.3 %copy-start.13 = (f32[512]{0:T(512)S(1)}, f32[512]{0:T(512)}, u32[]{:S(2)}) copy-start(f32[512]{0:T(512)} %param.31) | copy-start | bytes 6148
  44.9 11.3 %copy-start.15 = (f32[512]{0:T(512)S(1)}, f32[512]{0:T(512)}, u32[]{:S(2)}) copy-start(f32[512]{0:T(512)} %param.30) | copy-start | bytes 6148
  94.3 0.9 copy-start.1
  95.3 2.0 %copy-start.2 = (bf16[4608,384]{1,0:T(8,128)(2,1)S(1)}, bf16[4608,384]{1,0:T(8,128)(2,1)}, u32[]{:S(2)}) copy-start(bf16[4608,384]{1,0:T(8,128)(2,1)} %all-gather.6.cloned.1.call-done) | copy-start | bytes 10616836
  97.3 51.8 %copy-start.12 = (f32[512]{0:T(512)S(1)}, f32[512]{0:T(512)}, u32[]{:S(2)}) copy-start(f32[512]{0:T(512)} %param.32) | copy-start | bytes 6148
  149.1 1.1 copy-start.3
  149.1 1.1 copy-start.14
  149.1 1.1 copy-start.16
  149.1 1.9 %copy-start.19 = (bf16[512,2048]{1,0:T(8,128)(2,1)S(1)}, bf16[512,2048]{1,0:T(8,128)(2,1)}, u32[]{:S(2)}) copy-start(bf16[512,2048]{1,0:T(8,128)(2,1)} %param.35) | copy-start | bytes 6291460
  149.1 1.8 %copy-start.24 = (f32[512]{0:T(512)S(1)}, f32[512]{0:T(512)}, u32[]{:S(2)}) copy-start(f32[512]{0:T(512)} %param.33) | copy-start | bytes 6148
Sparse Core Ops, SparseCore 0:
  8.9 11.4 all-gather.3
  26.2 68.1 all-gather.5
  153.5 10.2 reduce-scatter.1

commit v2 on v1

--- a/solution.py
+++ b/solution.py
@@ -46,7 +46,384 @@
     )
 
 
-def attention_kernel(q_ref, lat_ref, kup_ref, vup_ref, o_ref, kt, vt, run_max, acc):
+MESH = pl.DeviceIdType.MESH
+
+
+def push(src, dst, send, recv, target):
+    return pltpu.make_async_remote_copy(
+        src_ref=src,
+        dst_ref=dst,
+        send_sem=send,
+        recv_sem=recv,
+        device_id=target,
+        device_id_type=MESH,
+    )
+
+
+def greet(targets):
+    barrier = pltpu.get_barrier_semaphore()
+    for target in targets:
+        pl.semaphore_signal(barrier, inc=1, device_id=target, device_id_type=MESH)
+    pl.semaphore_wait(barrier, len(targets))
+
+
+def other_core():
+    return {"sp": lax.axis_index("sp"), "tp": 1 - lax.axis_index("tp")}
+
+
+def tokens_kernel(tok_ref, gain_ref, scaled_ref, scale_ref, landed, send, recv):
+    mine = lax.axis_index("tp")
+    width = tok_ref.shape[1]
+    greet([other_core()])
+    copy = push(tok_ref, landed, send, recv, other_core())
+    copy.start()
+
+    def place(block, index):
+        cols = pl.ds(pl.multiple_of(index * width, 128), width)
+        wide = block[...].astype(jnp.float32)
+        scaled_ref[:, cols] = (wide * gain_ref[:, cols]).astype(jnp.bfloat16)
+        return jnp.sum(wide * wide, axis=1, keepdims=True)
+
+    squares = place(tok_ref, mine)
+    copy.wait()
+    squares = squares + place(landed, 1 - mine)
+    scale_ref[...] = lax.rsqrt(squares / (2 * width) + norm_eps)
+
+
+def exchange_tokens(tokens, gain):
+    rows, width = tokens.shape
+    vmem = pl.BlockSpec(memory_space=pltpu.VMEM)
+    return pl.pallas_call(
+        tokens_kernel,
+        out_shape=(
+            jax.ShapeDtypeStruct((rows, 2 * width), jnp.bfloat16),
+            jax.ShapeDtypeStruct((rows, 1), jnp.float32),
+        ),
+        in_specs=[vmem] * 2,
+        out_specs=(vmem, vmem),
+        scratch_shapes=[
+            pltpu.VMEM((rows, width), jnp.bfloat16),
+            pltpu.SemaphoreType.DMA,
+            pltpu.SemaphoreType.DMA,
+        ],
+        compiler_params=pltpu.CompilerParams(collective_id=0, has_side_effects=True),
+        name="token_exchange",
+    )(tokens, gain)
+
+
+def output_kernel(
+    att_ref, swish_ref, att_gain, conv_gain, att_w, conv_w, out_ref,
+    sq_mine, sq_other, part, landed, sq_send, sq_recv, send, recv,
+):
+    mine = lax.axis_index("tp")
+    rows, width = out_ref.shape
+    lanes = sq_mine.shape[1] // 2
+    attended = att_ref[...].astype(jnp.float32)
+    swished = swish_ref[...]
+    for slot, value in enumerate((attended, swished)):
+        total = jnp.sum(value * value, axis=1, keepdims=True)
+        sq_mine[:, slot * lanes : (slot + 1) * lanes] = jnp.broadcast_to(total, (rows, lanes))
+    greet([other_core()])
+    sums = push(sq_mine, sq_other, sq_send, sq_recv, other_core())
+    sums.start()
+    sums.wait()
+    sq = sq_mine[...] + sq_other[...]
+    att_scale = lax.rsqrt(sq[:, :1] / ATT_WIDTH + norm_eps)
+    conv_scale = lax.rsqrt(sq[:, lanes : lanes + 1] / CONV_CH + norm_eps)
+    att_mixed = (attended * att_scale * att_gain[...]).astype(jnp.bfloat16)
+    conv_mixed = (swished * conv_scale * conv_gain[...]).astype(jnp.bfloat16)
+    piece = part.shape[2]
+    pieces = part.shape[0]
+
+    def product(owner, index):
+        cols = pl.ds(pl.multiple_of(owner * width + index * piece, 128), piece)
+        return (
+            jnp.dot(att_mixed, att_w[:, cols], preferred_element_type=jnp.float32)
+            + jnp.dot(conv_mixed, conv_w[:, cols], preferred_element_type=jnp.float32)
+        ).astype(jnp.bfloat16)
+
+    copies = []
+    for index in range(pieces):
+        part[index] = product(1 - mine, index)
+        copy = push(
+            part.at[index], landed.at[index], send.at[index], recv.at[index], other_core()
+        )
+        copy.start()
+        copies.append(copy)
+    for index in range(pieces):
+        own = product(mine, index).astype(jnp.float32)
+        copies[index].wait()
+        out_ref[:, index * piece : (index + 1) * piece] = (
+            own + landed[index].astype(jnp.float32)
+        ).astype(jnp.bfloat16)
+
+
+def merge(attended, swished, att_gain, conv_gain, att_w, conv_w):
+    rows = attended.shape[0]
+    width = att_w.shape[1] // 2
+    pieces = 4
+    vmem = pl.BlockSpec(memory_space=pltpu.VMEM)
+    return pl.pallas_call(
+        output_kernel,
+        out_shape=jax.ShapeDtypeStruct((rows, width), jnp.bfloat16),
+        in_specs=[vmem] * 6,
+        out_specs=vmem,
+        scratch_shapes=[
+            pltpu.VMEM((rows, 256), jnp.float32),
+            pltpu.VMEM((rows, 256), jnp.float32),
+            pltpu.VMEM((pieces, rows, width // pieces), jnp.bfloat16),
+            pltpu.VMEM((pieces, rows, width // pieces), jnp.bfloat16),
+            pltpu.SemaphoreType.DMA,
+            pltpu.SemaphoreType.DMA,
+            pltpu.SemaphoreType.DMA((pieces,)),
+            pltpu.SemaphoreType.DMA((pieces,)),
+        ],
+        compiler_params=pltpu.CompilerParams(collective_id=1, has_side_effects=True),
+        name="output_merge",
+    )(attended, swished, att_gain, conv_gain, att_w, conv_w)
+
+
+PLANE = 4
+
+
+def attention_kernel(
+    q_ref, own_ref, kup_ref, vup_ref, o_ref, kt, vt, run_max, acc, lat_ref,
+    col_send, plane_send, core_send, link_recv, core_recv,
+):
+    heads, rows, lanes = q_ref.shape
+    blocks = lat_ref.shape[0]
+    rank = kup_ref.shape[1]
+    nope = kup_ref.shape[0] // heads
+    vdim = vup_ref.shape[0] // heads
+    rot = lat_ref.shape[1] - rank
+    wide = kt.shape[2]
+    pairing = wide // rows
+    me = lax.axis_index("sp")
+    core = lax.axis_index("tp")
+    layers = blocks // PLANE
+    layer = me // PLANE
+    spot = me % PLANE
+    last = me // pairing
+    height = lat_ref.shape[1] // 2
+    half = pl.ds(pl.multiple_of(core * height, 16), height)
+
+    def spot_at(distance):
+        return (spot + distance) % PLANE
+
+    def at(layer_id, spot_id):
+        return {"sp": layer_id * PLANE + spot_id, "tp": core}
+
+    greet(
+        [at((layer + d) % layers, spot) for d in range(1, layers)]
+        + [at(layer, spot_at(d)) for d in range(1, PLANE)]
+        + [other_core()]
+    )
+
+    def column_copy(distance):
+        return push(
+            own_ref.at[half],
+            lat_ref.at[me, half],
+            col_send.at[distance - 1],
+            link_recv.at[me],
+            at(jnp.minimum(layer + distance, layers - 1), spot),
+        )
+
+    def plane_copy(source, block, distance):
+        return push(
+            source,
+            lat_ref.at[block, half],
+            plane_send.at[block // PLANE, distance - 1],
+            link_recv.at[block],
+            at(layer, spot_at(distance)),
+        )
+
+    def core_copy(block):
+        spread = lat_ref.at[block, half]
+        return push(spread, spread, core_send.at[block], core_recv.at[block], other_core())
+
+    for d in range(1, PLANE):
+        plane_copy(own_ref.at[half], me, d).start()
+    for d in range(1, layers):
+
+        @pl.when(layer + d < layers)
+        def _(d=d):
+            column_copy(d).start()
+
+    lat_ref[me] = own_ref[...]
+
+    def relay(step):
+        @pl.when(step <= layer)
+        def _():
+            block = (layer - step) * PLANE + spot
+            landed(block)
+            for d in range(1, PLANE):
+                plane_copy(lat_ref.at[block, half], block, d).start()
+            core_copy(block).start()
+
+    def hand_over(step):
+        @pl.when(step <= layer)
+        def _():
+            for d in range(1, PLANE):
+                block = (layer - step) * PLANE + spot_at(d)
+                landed(block)
+                core_copy(block).start()
+
+    def landed(block):
+        spread = lat_ref.at[block, half]
+        push(spread, spread, core_send.at[block], link_recv.at[block], other_core()).wait_recv()
+
+    def gathered(step):
+        for d in range(1, PLANE):
+            core_copy((layer - step) * PLANE + spot_at(d)).wait_recv()
+
+    def expand(pair):
+        for part in range(pairing):
+            src = pair * pairing + part
+            lat = lat_ref[src, :rank, :]
+            turned = lat_ref[src, rank:, :]
+            cols = slice(part * rows, (part + 1) * rows)
+            keys = jnp.dot(kup_ref[...], lat, preferred_element_type=jnp.float32)
+            values = jnp.dot(vup_ref[...], lat, preferred_element_type=jnp.float32)
+            for head in range(heads):
+                kt[head, :nope, cols] = keys[head * nope : (head + 1) * nope].astype(jnp.bfloat16)
+                kt[head, nope : nope + rot, cols] = turned
+                vt[head, :vdim, cols] = values[head * vdim : (head + 1) * vdim].astype(
+                    jnp.bfloat16
+                )
+
+    def score(head):
+        return jnp.dot(q_ref[head], kt[head], preferred_element_type=jnp.float32)
+
+    def weigh(head, scores, top):
+        weights = jnp.exp2(scores - top).astype(jnp.bfloat16)
+        return lax.dot_general(
+            weights, vt[head], (((1,), (1,)), ((), ())), preferred_element_type=jnp.float32
+        )
+
+    def visit(pair):
+        expand(pair)
+        ahead = score(0)
+        for head in range(heads):
+            scores = ahead
+            if head + 1 < heads:
+                ahead = score(head + 1)
+            old = run_max[head]
+            top = jnp.maximum(old[:, :1], jnp.max(scores, axis=1, keepdims=True))
+            wide_top = jnp.broadcast_to(top, (rows, lanes))
+            run_max[head] = wide_top
+            acc[head] = acc[head] * jnp.exp2(old - wide_top) + weigh(head, scores, top)
+
+    kt[:, nope + rot :, :] = jnp.zeros((heads, lanes - nope - rot, wide), jnp.bfloat16)
+    vt[:, vdim:, :] = jnp.ones((heads, lanes - vdim, wide), jnp.bfloat16)
+    hand_over(0)
+    relay(1)
+    gathered(0)
+    expand(last)
+    key_pos = last * wide + lax.broadcasted_iota(jnp.int32, (rows, wide), 1)
+    query_pos = me * rows + lax.broadcasted_iota(jnp.int32, (rows, wide), 0)
+    hidden = key_pos > query_pos
+    ahead = score(0)
+    for head in range(heads):
+        scores = jnp.where(hidden, far_below, ahead)
+        if head + 1 < heads:
+            ahead = score(head + 1)
+        top = jnp.max(scores, axis=1, keepdims=True)
+        run_max[head] = jnp.broadcast_to(top, (rows, lanes))
+        acc[head] = weigh(head, scores, top)
+    hand_over(1)
+    relay(2)
+
+    per_layer = PLANE // pairing
+    first = layer * per_layer
+
+    def near(step, carry):
+        visit(last - 1 - step)
+        return carry
+
+    lax.fori_loop(0, last - first, near, 0)
+
+    def far(step, carry):
+        gathered_all(step)
+
+        def one(turn, inner):
+            @pl.when(turn == 1)
+            def _():
+                hand_over(step + 1)
+                relay(step + 2)
+
+            visit((layer - step) * per_layer + per_layer - 1 - turn)
+            return inner
+
+        lax.fori_loop(0, per_layer, one, 0)
+        return carry
+
+    def gathered_all(step):
+        for d in range(PLANE):
+            core_copy((layer - step) * PLANE + spot_at(d)).wait_recv()
+
+    lax.fori_loop(1, layer + 1, far, 0)
+    lane = lax.broadcasted_iota(jnp.int32, (rows, lanes), 1)
+    for pair in range(heads // 2):
+        halves = []
+        for head in (2 * pair, 2 * pair + 1):
+            total = acc[head]
+            halves.append(total / pltpu.roll(total, vdim, axis=1))
+        both = jnp.where(lane < vdim, halves[0], pltpu.roll(halves[1], vdim, axis=1))
+        o_ref[:, pair * lanes : (pair + 1) * lanes] = both.astype(jnp.bfloat16)
+
+    for d in range(1, layers):
+
+        @pl.when(layer + d < layers)
+        def _(d=d):
+            column_copy(d).wait_send()
+
+    def settle(step, carry):
+        base = (layer - step) * PLANE
+        for d in range(1, PLANE):
+            plane_copy(own_ref.at[half], base + spot, d).wait_send()
+            core_copy(base + spot_at(d)).wait_send()
+
+        @pl.when(step > 0)
+        def _():
+            core_copy(base + spot).wait_send()
+
+        return carry
+
+    lax.fori_loop(0, layer + 1, settle, 0)
+
+
+def attention(q_heads, packed, key_up_t, value_up_t):
+    heads, rows, lanes = q_heads.shape
+    blocks = lax.axis_size("sp")
+    wide = 2 * rows
+    layers = blocks // PLANE
+    vmem = pl.BlockSpec(memory_space=pltpu.VMEM)
+    dma = pltpu.SemaphoreType.DMA
+    return pl.pallas_call(
+        attention_kernel,
+        out_shape=jax.ShapeDtypeStruct((rows, value_up_t.shape[0]), jnp.bfloat16),
+        in_specs=[vmem] * 4,
+        out_specs=vmem,
+        scratch_shapes=[
+            pltpu.VMEM((heads, lanes, wide), jnp.bfloat16),
+            pltpu.VMEM((heads, lanes, wide), jnp.bfloat16),
+            pltpu.VMEM((heads, rows, lanes), jnp.float32),
+            pltpu.VMEM((heads, rows, lanes), jnp.float32),
+            pltpu.VMEM((blocks,) + packed.shape, jnp.bfloat16),
+            dma((max(layers - 1, 1),)),
+            dma((layers, PLANE - 1)),
+            dma((blocks,)),
+            dma((blocks,)),
+            dma((blocks,)),
+        ],
+        compiler_params=pltpu.CompilerParams(
+            vmem_limit_bytes=56 << 20, collective_id=2, has_side_effects=True
+        ),
+        name="attention",
+    )(q_heads, packed, key_up_t, value_up_t)
+
+
+def gathered_kernel(q_ref, lat_ref, kup_ref, vup_ref, o_ref, kt, vt, run_max, acc):
     heads, rows, lanes = q_ref.shape
     blocks = lat_ref.shape[0]
     rank = kup_ref.shape[1]
@@ -114,13 +491,13 @@
         o_ref[:, pair * lanes : (pair + 1) * lanes] = both.astype(jnp.bfloat16)
 
 
-def attention(q_heads, lat_all, key_up_t, value_up_t):
+def gathered_attention(q_heads, lat_all, key_up_t, value_up_t):
     heads, rows, lanes = q_heads.shape
     blocks = lat_all.shape[0]
     wide = 2 * rows if blocks % 2 == 0 else rows
     vmem = pl.BlockSpec(memory_space=pltpu.VMEM)
     return pl.pallas_call(
-        attention_kernel,
+        gathered_kernel,
         out_shape=jax.ShapeDtypeStruct((rows, value_up_t.shape[0]), jnp.bfloat16),
         in_specs=[vmem] * 4,
         out_specs=vmem,
@@ -134,7 +511,7 @@
         cost_estimate=pl.CostEstimate(
             flops=20_000_000_000, bytes_accessed=8 << 20, transcendentals=20_000_000
         ),
-        name="attention",
+        name="gathered_attention",
     )(q_heads, lat_all, key_up_t, value_up_t)
 
 
@@ -209,17 +586,21 @@
         conv_value_weight,
         conv_gate_weight,
     )
-    wide_part = lax.all_gather(tokens, "tp", axis=1, tiled=True).astype(jnp.float32)
-    scaled = (wide_part * input_gain[None, :]).astype(jnp.bfloat16)
+    paired = lax.axis_size("tp") == 2 and lax.axis_size("sp") % PLANE == 0
+    if paired:
+        scaled, row_scale = exchange_tokens(tokens, input_gain[None, :])
+    else:
+        whole_rows = lax.all_gather(tokens, "tp", axis=1, tiled=True).astype(jnp.float32)
+        scaled = (whole_rows * input_gain[None, :]).astype(jnp.bfloat16)
+        row_scale = lax.rsqrt(
+            jnp.mean(whole_rows * whole_rows, axis=1, keepdims=True) + norm_eps
+        )
 
     def add_product(weight):
         return jnp.dot(scaled, weight, preferred_element_type=jnp.float32)
 
     summed = tuple((add_product(weight) for weight in weight_list))
-    q_acc, qrot_acc, latent_raw, rot_acc, value_acc, gate_acc, square_sum = summed + (
-        jnp.sum(wide_part * wide_part, axis=1),
-    )
-    row_scale = lax.rsqrt(square_sum / D_MODEL + norm_eps)[:, None]
+    q_acc, qrot_acc, latent_raw, rot_acc, value_acc, gate_acc = summed
     positions = lax.axis_index("sp") * tok_rows + jnp.arange(tok_rows, dtype=jnp.int32)
     cos_table, sine_table = rotary_tables(positions, ROT_DIM // 2)
     fold = math.log2(math.e) / math.sqrt(NOPE_DIM + ROT_DIM)
@@ -243,16 +624,9 @@
     gated_input = (value_acc * row_scale * jax.nn.sigmoid(gate_acc * row_scale)).astype(
         jnp.bfloat16
     )
-    def square_rows(matrix):
-        wide_rows = matrix.astype(jnp.float32)
-        return jnp.sum(wide_rows * wide_rows, axis=1)
-
     packed = jnp.concatenate([latent.T, key_rot.T], axis=0)
-    lat_all = lax.all_gather(packed, "sp", axis=0)
     rim_rows = shifted(gated_input[tok_rows - (KERNEL + 1) :], "sp", 1)
     conv_out = convolve(gated_input, rim_rows, conv_taps)
-    attended = attention(q_heads, lat_all, key_up.T, value_up.T)
-    att_sq = lax.psum(square_rows(attended), "tp")
     moment_one, moment_two = lax.psum(
         (jnp.sum(conv_out, axis=1), jnp.sum(conv_out * conv_out, axis=1)), "tp"
     )
@@ -260,28 +634,36 @@
     spread = moment_two / CONV_CH - mean_val * mean_val
     normed = (conv_out - mean_val[:, None]) * lax.rsqrt(spread + norm_eps)[:, None]
     swished = jax.nn.silu(normed * conv_ln_gain[None, :] + conv_ln_bias[None, :])
-    conv_sq = lax.psum(square_rows(swished), "tp")
+    if paired:
+        attended = attention(q_heads, packed, key_up.T, value_up.T)
+        return merge(
+            attended,
+            swished,
+            att_out_gain[None, :],
+            conv_out_gain[None, :],
+            att_out_weight,
+            conv_out_weight,
+        )
+    lat_all = lax.all_gather(packed, "sp", axis=0)
+    attended = gathered_attention(q_heads, lat_all, key_up.T, value_up.T).astype(jnp.float32)
+    att_sq, conv_sq = lax.psum(
+        (
+            jnp.sum(attended * attended, axis=1, keepdims=True),
+            jnp.sum(swished * swished, axis=1, keepdims=True),
+        ),
+        "tp",
+    )
     att_mixed = (
-        attended.astype(jnp.float32)
-        * lax.rsqrt(att_sq / ATT_WIDTH + norm_eps)[:, None]
-        * att_out_gain[None, :]
+        attended * lax.rsqrt(att_sq / ATT_WIDTH + norm_eps) * att_out_gain[None, :]
     ).astype(jnp.bfloat16)
     conv_mixed = (
-        swished * lax.rsqrt(conv_sq / CONV_CH + norm_eps)[:, None] * conv_out_gain[None, :]
+        swished * lax.rsqrt(conv_sq / CONV_CH + norm_eps) * conv_out_gain[None, :]
     ).astype(jnp.bfloat16)
-    contract = (((0,), (1,)), ((), ()))
-    feature_rows = lax.psum_scatter(
-        (
-            lax.dot_general(att_out_weight, att_mixed, contract, preferred_element_type=jnp.float32)
-            + lax.dot_general(
-                conv_out_weight, conv_mixed, contract, preferred_element_type=jnp.float32
-            )
-        ).astype(jnp.bfloat16),
-        "tp",
-        scatter_dimension=0,
-        tiled=True,
-    ).astype(jnp.float32)
-    return feature_rows.T.astype(jnp.bfloat16)
+    share = (
+        jnp.dot(att_mixed, att_out_weight, preferred_element_type=jnp.float32)
+        + jnp.dot(conv_mixed, conv_out_weight, preferred_element_type=jnp.float32)
+    ).astype(jnp.bfloat16)
+    return lax.psum_scatter(share, "tp", scatter_dimension=1, tiled=True)
 
 
 def solution(mesh):

time: 172 us -> 103 us (0.60)
  waiting for transfers between devices: 62.9 us -> 0.01 us
  Pallas kernels: 52.2 us -> 67.2 us
  between operations: 13.5 us -> 0.32 us
  matrix products: 16 us -> 12 us
  blocking collectives: 7.12 us -> 3.53 us
    all_gather x2 -> x0, waiting for transfers between devices: 49.5 us -> none  [the longest x1 36.5 us: shards(): lat_all = lax.all_gather(packed, 'sp', axis=0)]
    pallas_call x0 -> x2, Pallas kernels: none -> 15.7 us  [the longest x1 10.3 us: merge(): pl.pallas_call(output_kernel, out_shape=jax.ShapeDtypeStruct((rows, width...]
    reduce_scatter x1 -> x0, waiting for transfers between devices: 10.4 us -> none  [shards(): lax.psum_scatter((lax.dot_general(att_out_weight, att_mixed, contract, pr...]
    reduce_sum x3 -> x0, other arithmetic: 3.66 us -> none  [the longest x1 1.91 us: shards(): jnp.sum(wide_part * wide_part, axis=1)]
    dot_general x2 -> x0, matrix products: 3.46 us -> none  [the longest x1 2.43 us: shards(): lax.dot_general(conv_out_weight, conv_mixed, contract, preferred_element_...]
    psum x1 -> x0, blocking collectives: 3.45 us -> none  [shards(): att_sq = lax.psum(square_rows(attended), 'tp')]
    mul x0 -> x1, other arithmetic: none -> 2.38 us  [shards(): jax.nn.silu(normed * conv_ln_gain[None, :] + conv_ln_bias[None, :])]
    ppermute x1, waiting for transfers between devices: 2.19 us -> 0.01 us  [shifted(): return lax.ppermute(block, axis, route)]
  transfers between devices with their start and end apart: 4 -> 1, of which waited for: 4 -> 0; matrix products, arithmetic and copies ran while one was open for 12% -> 19% of each run, Pallas kernels for 2% -> 46%
where the time goes in v2:
time: 103 us; the launch traced here: 102 us
  Pallas kernels  67.2 us (65%)
  matrix products  12 us (12%)
  local copies, waits for them, and re-layouts  10.3 us (10%)
  other arithmetic  7.89 us (8%)
  blocking collectives  3.53 us (3%)
  starting transfers between devices  1.28 us (1%)
    pallas_call x1, Pallas kernels, attention(): pl.pallas_call(attention_kernel, out_shape=jax.ShapeDtypeStruct((rows, va...  47.4 us
    dot_general x6, matrix products, add_product(): return jnp.dot(scaled, weight, preferred_element_type=jnp.float32)  12 us
    pallas_call x1, Pallas kernels, merge(): pl.pallas_call(output_kernel, out_shape=jax.ShapeDtypeStruct((rows, width...  10.3 us
    unnamed x31, local copies, waits for them, and re-layouts  8.01 us
    pallas_call x1, Pallas kernels, exchange_tokens(): pl.pallas_call(tokens_kernel, out_shape=(jax.ShapeDtypeStruct((rows, 2 *...  5.35 us
    pallas_call x1, Pallas kernels, convolve(): pl.pallas_call(conv_kernel, out_shape=jax.ShapeDtypeStruct((rows, chans),...  4.06 us
    psum x1, blocking collectives, shards(): lax.psum((jnp.sum(conv_out, axis=1), jnp.sum(conv_out * conv_out, axis=1)...  3.53 us
    mul x1, other arithmetic, shards(): jax.nn.silu(normed * conv_ln_gain[None, :] + conv_ln_bias[None, :])  2.38 us
  transfers between devices with their start and end apart: 1, of which 0 were waited for; matrix products, arithmetic and copies ran while one was open for 19% of the time, Pallas kernels for 46%

profile of v2, /device:TPU:31, one launch (start us, length us, event | category | flops | bytes accessed | tf_op | source)
XLA Modules:
  0.0 102.5 jit_solution(435579810729057737)
XLA Ops:
  0.0 0.0 copy-start
  0.0 5.4 %token_exchange.1 = (bf16[384,2048]{1,0:T(8,128)(2,1)}, f32[384,1]{1,0:T(8,128)}) custom-call(bf16[384,1024]{1,0:T(8,128)(2,1)} %tok_ref.1, f32[1,2048]{1,0:T(1,128)} %bitcast.29), custom_call_target="tpu_custom_call" | custom-call | tf_op jit(solution)/shard_map/token_exchange/pallas_call | solution.py:96
  5.4 1.1 %fusion.9 = (f32[384]{0:T(512)S(1)}, f32[384]{0:T(512)S(1)}) fusion(f32[384,1]{1,0:T(8,128)} %get-tuple-element.8), kind=kLoop, calls=%fused_computation.33 | loop fusion | flops 384 | bytes 4608 | tf_op jit(solution)/shard_map/token_exchange/pallas_call | solution.py:96
  6.5 0.0 copy-done
  6.5 0.0 copy-start.1
  6.5 0.0 copy-start.12
  6.5 2.6 %fusion.4 = f32[384,512]{1,0:T(8,128)S(1)} fusion(bf16[384,2048]{1,0:T(8,128)(2,1)} %get-tuple-element.7, bf16[2048,512]{1,0:T(8,128)(2,1)S(1)} %copy-done, f32[384]{0:T(512)S(1)} %get-tuple-element.11), kind=kOutput, calls=%fused_computation.9 | convolution fusion | flops 806092800 | bytes 4457984 | tf_op jit(solution)/shard_map/dot_general | solution.py:600
  9.2 0.0 copy-done.1
  9.2 0.0 copy-done.12
  9.2 0.0 copy-start.4
  9.2 1.0 fusion.6.gated_ref
  10.2 0.0 copy-start.6
  10.2 0.6 slice.24
  10.8 1.3 %collective-permute-start = (bf16[32,512]{1,0:T(8,128)(2,1)}, bf16[32,512]{1,0:T(8,128)(2,1)}, u32[]{:S(2)}, u32[]{:S(2)}) collective-permute-start(bf16[32,512]{1,0:T(8,128)(2,1)} %slice.24), channel_id=1, source_target_pairs={{0,2},{2,4},{4,6},{6,8},{8,10},{10,12},{12,14},{14,16},{16,18},{18... | collective-permute-start | bytes 98312 | tf_op jit(solution)/shard_map/ppermute | solution.py:27
  12.1 0.0 copy-done.6
  12.1 0.0 copy-done.4
  12.2 0.8 convolution_multiply_fusion.3
  13.0 0.0 copy-start.8
  13.0 1.6 %copy.32 = f32[384,8,16]{2,0,1:T(8,128)} copy(f32[384,8,16]{0,2,1:T(8,128)S(1)} %get-tuple-element.17) | data formatting | bytes 393216
  14.6 1.6 %copy.31 = f32[384,8,16]{2,0,1:T(8,128)} copy(f32[384,8,16]{0,2,1:T(8,128)S(1)} %get-tuple-element.18) | data formatting | bytes 393216
  16.2 0.0 copy-done.8
  16.2 2.0 %convolution_multiply_fusion.4 = f32[384,32]{0,1:T(8,128)S(1)} fusion(bf16[384,2048]{1,0:T(8,128)(2,1)} %get-tuple-element.7, bf16[2048,32]{0,1:T(8,128)(2,1)S(1)} %copy-done.8, f32[384]{0:T(512)S(1)} %get-tuple-element.11), kind=kOutput, calls=%fused_computation.13 | convolution fusion | flops 50343936 | bytes 1754624 | tf_op jit(solution)/shard_map/dot_general | solution.py:600
  18.2 0.2 subtract_convert_fusion.1
  18.4 0.1 copy.27
  18.5 0.8 copy.25
  19.4 3.0 %fusion.5 = bf16[384,512]{1,0:T(8,128)(2,1)S(1)} fusion(bf16[384,2048]{1,0:T(8,128)(2,1)} %get-tuple-element.7, bf16[2048,512]{1,0:T(8,128)(2,1)} %param.20, f32[384]{0:T(512)S(1)} %get-tuple-element.12), kind=kOutput, calls=%fused_computation.10 | convolution fusion | flops 805699584 | bytes 4064768 | tf_op jit(solution)/shard_map/dot_general | solution.py:600
  22.4 0.2 copy.23
  22.6 0.0 copy-start.11
  22.6 0.4 copy.28
  23.0 0.0 copy-start.2
  23.0 0.0 copy-start.3
  23.0 0.0 copy-start.5
  23.1 2.6 %multiply_reduce_fusion.1 = (f32[384]{0:T(512)S(1)}, f32[384,256]{0,1:T(8,128)S(1)}) fusion(bf16[384,2048]{1,0:T(8,128)(2,1)} %get-tuple-element.7, bf16[2048,256]{1,0:T(8,128)(2,1)} %param.22), kind=kOutput, calls=%fused_computation.18 | convolution fusion | flops 402849408 | bytes 3016192 | tf_op jit(solution)/shard_map/dot_general | solution.py:600
  25.7 0.1 pad.7.clone
  25.8 0.0 copy-done.11
  25.8 0.1 fusion.7
  25.9 0.0 copy-done.2
  25.9 0.0 copy-done.3
  25.9 0.0 copy-done.5
  25.9 0.4 subtract_convert_fusion
  26.4 0.0 copy-start.7
  26.4 1.6 %maximum_bitcast_fusion.q_ref = bf16[8,384,128]{2,1,0:T(8,128)(2,1)} fusion(bf16[384,8,16]{2,0,1:T(8,128)(2,1)S(1)} %get-tuple-element.16, bf16[384,8,16]{2,0,1:T(8,128)(2,1)S(1)} %get-tuple-element.15, bf16[384,8,64]{2,0,1:T(8,128)(2,1)S(1)} %copy.28, bf16[128]{0:T(256)(128)(2,1)S(1)} %pad.7.clone), kind=kLoop, calls=%fused_computation.14 | loop fusion | flops 3145728 | bytes 1376512 | tf_op jit(solution)/shard_map/transpose | solution.py:615
  28.0 0.7 pad_maximum_fusion.own_ref
  28.7 0.0 copy-done.7
  28.7 0.8 copy.29
  29.6 1.8 %copy.30 = bf16[256,512]{0,1:T(8,128)(2,1)} copy(bf16[256,512]{1,0:T(8,128)(2,1)} %param.26) | data formatting | bytes 524288 | tf_op args[8]
  31.3 0.0 copy-start.9
  31.3 0.0 copy-start.10
  31.3 47.4 %attention.1.att_ref = bf16[384,512]{1,0:T(8,128)(2,1)} custom-call(bf16[8,384,128]{2,1,0:T(8,128)(2,1)} %maximum_bitcast_fusion.q_ref, bf16[288,384]{1,0:T(8,128)(2,1)} %pad_maximum_fusion.own_ref, bf16[512,256]{1,0:T(8,128)(2,1)} %bitcast.27, bf16[512,256]{1,0:T(8,128)(2,1)} %bitcast.28), custom_call_target="tpu_custom_call" | custom-call | tf_op jit(solution)/shard_map/attention/pallas_call | solution.py:402
  78.8 0.0 collective-permute-done.rim_ref
  78.8 4.1 %depthwise.1 = f32[384,512]{1,0:T(8,128)} custom-call(bf16[384,512]{1,0:T(8,128)(2,1)} %copy-done.6, bf16[32,512]{1,0:T(8,128)(2,1)} %collective-permute-done.rim_ref, f32[31,512]{1,0:T(8,128)} %taps_ref.1), custom_call_target="tpu_custom_call" | custom-call | flops 12189696 | bytes 2097152 | tf_op jit(solution)/shard_map/depthwise/pallas_call | solution.py:545
  82.8 1.3 %fusion.8 = (f32[384]{0:T(512)S(1)}, f32[384]{0:T(512)S(1)}) fusion(f32[384,512]{1,0:T(8,128)} %depthwise.1), kind=kLoop, calls=%fused_computation.32 | loop fusion | flops 589056 | bytes 789504 | tf_op jit(solution)/shard_map/reduce_sum | solution.py:631
  84.1 3.5 %all-reduce = (f32[384]{0:T(512)S(1)}, f32[384]{0:T(512)S(1)}) all-reduce(f32[384]{0:T(512)S(1)} %get-tuple-element.10, f32[384]{0:T(512)S(1)} %get-tuple-element.9), channel_id=1, replica_groups=mesh['sp'=16,'tp'=2] {'tp'}, use_global_device_ids=true, to_apply=%region_4.0 | all-reduce | flops 768 | bytes 6144 | tf_op jit(solution)/shard_map/psum | solution.py:630
  87.7 0.0 copy-done.9
  87.7 0.0 copy-done.10
  87.7 2.4 %divide_multiply_fusion.swish_ref = f32[384,512]{1,0:T(8,128)} fusion(f32[384,512]{1,0:T(8,128)} %depthwise.1, f32[512]{0:T(512)S(1)} %copy-done.9, f32[512]{0:T(512)S(1)} %copy-done.10, f32[384]{0:T(512)S(1)} %get-tuple-element.24, f32[384]{0:T(512)S(1)} %get-tuple-element.23), kind=kLoop, calls=%fused_computation.15 | loop fusion | flops 1572864 | bytes 1580032 | tf_op jit(solution)/shard_map/jit(silu)/mul | solution.py:636
  90.1 10.3 %output_merge.1 = bf16[384,1024]{1,0:T(8,128)(2,1)} custom-call(bf16[384,512]{1,0:T(8,128)(2,1)} %attention.1.att_ref, f32[384,512]{1,0:T(8,128)} %divide_multiply_fusion.swish_ref, f32[1,512]{1,0:T(1,128)} %bitcast.30, f32[1,512]{1,0:T(1,128)} %bitcast.31, bf16[512,2048]{1,0:T(8,128)(2,1)} %att_w.1, bf16[512,2048]{1,0:T(8,128)(2,1)} %conv_w.1), custom_call_target="tpu_custom_call" | custom-call | tf_op jit(solution)/shard_map/output_merge/pallas_call | solution.py:166
  100.4 2.1 %copy.34 = bf16[384,1024]{1,0:T(8,128)(2,1)} copy(bf16[384,1024]{1,0:T(8,128)(2,1)} %output_merge.1) | data formatting | bytes 1572864
  (7 shorter events, 0.1 us)
Async XLA Ops:
  0.0 6.5 %copy-start = (bf16[2048,512]{1,0:T(8,128)(2,1)S(1)}, bf16[2048,512]{1,0:T(8,128)(2,1)}, u32[]{:S(2)}) copy-start(bf16[2048,512]{1,0:T(8,128)(2,1)} %param.28) | copy-start | bytes 6291460
  6.5 2.7 %copy-start.1 = (bf16[384,2048]{1,0:T(8,128)(2,1)S(1)}, bf16[384,2048]{1,0:T(8,128)(2,1)}, u32[]{:S(2)}) copy-start(bf16[384,2048]{1,0:T(8,128)(2,1)} %get-tuple-element.7) | copy-start | bytes 4718596
  6.5 2.7 %copy-start.12 = (bf16[2048,512]{1,0:T(8,128)(2,1)S(1)}, bf16[2048,512]{1,0:T(8,128)(2,1)}, u32[]{:S(2)}) copy-start(bf16[2048,512]{1,0:T(8,128)(2,1)} %param.27) | copy-start | bytes 6291460
  9.2 3.0 %copy-start.4 = (bf16[2048,256]{1,0:T(8,128)(2,1)S(1)}, bf16[2048,256]{1,0:T(8,128)(2,1)}, u32[]{:S(2)}) copy-start(bf16[2048,256]{1,0:T(8,128)(2,1)} %param.21) | copy-start | bytes 3145732
  10.2 2.0 %copy-start.6 = (bf16[384,512]{1,0:T(8,128)(2,1)}, bf16[384,512]{1,0:T(8,128)(2,1)S(1)}, u32[]{:S(2)}) copy-start(bf16[384,512]{1,0:T(8,128)(2,1)S(1)} %fusion.6.gated_ref) | copy-start | bytes 1179652
  10.8 67.9 %collective-permute-start = (bf16[32,512]{1,0:T(8,128)(2,1)}, bf16[32,512]{1,0:T(8,128)(2,1)}, u32[]{:S(2)}, u32[]{:S(2)}) collective-permute-start(bf16[32,512]{1,0:T(8,128)(2,1)} %slice.24), channel_id=1, source_target_pairs={{0,2},{2,4},{4,6},{6,8},{8,10},{10,12},{12,14},{14,16},{16,18},{18... | collective-permute-start | bytes 98312 | tf_op jit(solution)/shard_map/ppermute | solution.py:27
  13.0 3.3 %copy-start.8 = (bf16[2048,32]{0,1:T(8,128)(2,1)S(1)}, bf16[2048,32]{0,1:T(8,128)(2,1)}, u32[]{:S(2)}) copy-start(bf16[2048,32]{0,1:T(8,128)(2,1)} %param.23) | copy-start | bytes 393220
  22.6 3.2 %copy-start.11 = (f32[256]{0:T(256)S(1)}, f32[256]{0:T(256)}, u32[]{:S(2)}) copy-start(f32[256]{0:T(256)} %param.24) | copy-start | bytes 3076
  23.0 2.9 %copy-start.2 = (f32[384,8,16]{2,0,1:T(8,128)S(1)}, f32[384,8,16]{2,0,1:T(8,128)}, u32[]{:S(2)}) copy-start(f32[384,8,16]{2,0,1:T(8,128)} %copy.32) | copy-start | bytes 589828
  23.0 2.9 %copy-start.3 = (f32[384,8,16]{2,0,1:T(8,128)S(1)}, f32[384,8,16]{2,0,1:T(8,128)}, u32[]{:S(2)}) copy-start(f32[384,8,16]{2,0,1:T(8,128)} %copy.31) | copy-start | bytes 589828
  23.0 2.9 %copy-start.5 = (f32[384,16]{1,0:T(8,128)S(1)}, f32[384,16]{1,0:T(8,128)}, u32[]{:S(2)}) copy-start(f32[384,16]{1,0:T(8,128)} %copy.25) | copy-start | bytes 73732
  26.4 2.4 %copy-start.7 = (bf16[256,512]{1,0:T(8,128)(2,1)S(1)}, bf16[256,512]{1,0:T(8,128)(2,1)}, u32[]{:S(2)}) copy-start(bf16[256,512]{1,0:T(8,128)(2,1)} %param.25) | copy-start | bytes 786436
  31.3 56.3 %copy-start.9 = (f32[512]{0:T(512)S(1)}, f32[512]{0:T(512)}, u32[]{:S(2)}) copy-start(f32[512]{0:T(512)} %param.31) | copy-start | bytes 6148
  31.3 56.3 %copy-start.10 = (f32[512]{0:T(512)S(1)}, f32[512]{0:T(512)}, u32[]{:S(2)}) copy-start(f32[512]{0:T(512)} %param.30) | copy-start | bytes 6148

commit v3 on v2

--- a/solution.py
+++ b/solution.py
@@ -71,50 +71,197 @@
     return {"sp": lax.axis_index("sp"), "tp": 1 - lax.axis_index("tp")}
 
 
-def tokens_kernel(tok_ref, gain_ref, scaled_ref, scale_ref, landed, send, recv):
+def front_kernel(
+    tok_ref, gain_ref, kv_gain_ref, cos_ref, sin_ref, taps_ref, ln_gain_ref, ln_bias_ref,
+    qw_hbm, qrw_hbm, kvd_hbm, rotw_hbm, cvw_hbm, cgw_hbm,
+    q_ref, packed_ref, swish_ref,
+    qw, qrw, kvd, rotw, cvw, cgw, scaled, landed, narrow, gated, rim, wide, conv,
+    sq_mine, sq_other, w_sem, tok_send, tok_recv, rim_send, rim_recv, sq_send, sq_recv,
+):
     mine = lax.axis_index("tp")
-    width = tok_ref.shape[1]
-    greet([other_core()])
-    copy = push(tok_ref, landed, send, recv, other_core())
+    seat = lax.axis_index("sp")
+    seats = lax.axis_size("sp")
+    rows, width = tok_ref.shape
+    heads, _, lanes = q_ref.shape
+    loads = [
+        pltpu.make_async_copy(src, dst, w_sem.at[index])
+        for index, (src, dst) in enumerate(
+            (
+                (kvd_hbm, kvd), (rotw_hbm, rotw), (cvw_hbm, cvw),
+                (cgw_hbm, cgw), (qw_hbm, qw), (qrw_hbm, qrw),
+            )
+        )
+    ]
+    for load in loads:
+        load.start()
+    ahead = {"sp": (seat + 1) % seats, "tp": mine}
+    behind = {"sp": (seat + seats - 1) % seats, "tp": mine}
+    greet([other_core(), ahead, behind])
+    copy = push(tok_ref, landed, tok_send, tok_recv, other_core())
     copy.start()
 
     def place(block, index):
         cols = pl.ds(pl.multiple_of(index * width, 128), width)
-        wide = block[...].astype(jnp.float32)
-        scaled_ref[:, cols] = (wide * gain_ref[:, cols]).astype(jnp.bfloat16)
-        return jnp.sum(wide * wide, axis=1, keepdims=True)
+        full = block[...].astype(jnp.float32)
+        scaled[:, cols] = (full * gain_ref[:, cols]).astype(jnp.bfloat16)
+        return jnp.sum(full * full, axis=1, keepdims=True)
 
     squares = place(tok_ref, mine)
     copy.wait()
     squares = squares + place(landed, 1 - mine)
-    scale_ref[...] = lax.rsqrt(squares / (2 * width) + norm_eps)
-
-
-def exchange_tokens(tokens, gain):
+    row_scale = lax.rsqrt(squares / (2 * width) + norm_eps)
+
+    def project(weight):
+        return jnp.dot(scaled[...], weight[...], preferred_element_type=jnp.float32)
+
+    loads[2].wait()
+    loads[3].wait()
+    gate = project(cgw) * row_scale
+    gated[...] = (project(cvw) * row_scale * jax.nn.sigmoid(gate)).astype(jnp.bfloat16)
+    edge = rim.shape[0]
+    rim_copy = push(gated.at[pl.ds(rows - edge, edge)], rim, rim_send, rim_recv, ahead)
+
+    @pl.when(seat < seats - 1)
+    def _():
+        rim_copy.start()
+
+    loads[0].wait()
+    loads[1].wait()
+    raw = project(kvd)
+    rank = raw.shape[1]
+    latent = (
+        raw
+        * lax.rsqrt(jnp.mean(raw * raw, axis=1, keepdims=True) + norm_eps)
+        * kv_gain_ref[...]
+    )
+    packed_ref[:rank, :] = latent.T.astype(jnp.bfloat16)
+    cos_table = cos_ref[...]
+    sin_table = sin_ref[...]
+    turn = cos_table.shape[0]
+
+    def rotate(block):
+        front = block[:turn]
+        back = block[turn : 2 * turn]
+        return jnp.concatenate(
+            [front * cos_table - back * sin_table, back * cos_table + front * sin_table], axis=0
+        )
+
+    narrow[...] = jnp.zeros(narrow.shape, jnp.float32)
+    narrow[:, : 2 * turn] = project(rotw) * row_scale
+    packed_ref[rank:, :] = rotate(narrow[...].T).astype(jnp.bfloat16)
+    loads[4].wait()
+    loads[5].wait()
+    query_scale = row_scale * (math.log2(math.e) / math.sqrt(NOPE_DIM + ROT_DIM))
+    plain = (project(qw) * query_scale).T
+    turned = (project(qrw) * query_scale).T
+    blank = jnp.zeros((lanes - NOPE_DIM - ROT_DIM, rows), jnp.float32)
+    for head in range(heads):
+        column = jnp.concatenate(
+            [
+                plain[head * NOPE_DIM : (head + 1) * NOPE_DIM],
+                rotate(turned[head * ROT_DIM : (head + 1) * ROT_DIM]),
+                blank,
+            ],
+            axis=0,
+        )
+        q_ref[head] = column.T.astype(jnp.bfloat16)
+
+    @pl.when(seat > 0)
+    def _():
+        rim_copy.wait_recv()
+
+    @pl.when(seat == 0)
+    def _():
+        rim[...] = jnp.zeros(rim.shape, jnp.bfloat16)
+
+    taps = taps_ref.shape[0]
+    chunk = 64
+    for part in range(conv.shape[1] // 128):
+        cols = slice(part * 128, (part + 1) * 128)
+        wide[part, :edge, :] = rim[:, cols].astype(jnp.float32)
+        wide[part, edge:, :] = gated[:, cols].astype(jnp.float32)
+        coeff = taps_ref[:, cols]
+
+        def band(step, carry, part=part, cols=cols, coeff=coeff):
+            base = step * chunk
+            total = jnp.zeros((chunk, 128), jnp.float32)
+            for tap in range(taps):
+                total = total + coeff[tap : tap + 1, :] * wide[
+                    part, pl.ds(base + (edge - taps + 1 + tap), chunk), :
+                ]
+            conv[pl.ds(pl.multiple_of(base, chunk), chunk), cols] = total
+            return carry
+
+        lax.fori_loop(0, rows // chunk, band, 0)
+
+    values = conv[...]
+    for slot, total in enumerate((values, values * values)):
+        sq_mine[:, slot * 128 : (slot + 1) * 128] = jnp.broadcast_to(
+            jnp.sum(total, axis=1, keepdims=True), (rows, 128)
+        )
+    sums = push(sq_mine, sq_other, sq_send, sq_recv, other_core())
+    sums.start()
+    sums.wait()
+    moments = (sq_mine[...] + sq_other[...]) / CONV_CH
+    mean_val = moments[:, :1]
+    spread = moments[:, 128:129] - mean_val * mean_val
+    normed = (values - mean_val) * lax.rsqrt(spread + norm_eps)
+    swish_ref[...] = jax.nn.silu(normed * ln_gain_ref[...] + ln_bias_ref[...])
+
+    @pl.when(seat < seats - 1)
+    def _():
+        rim_copy.wait_send()
+
+
+def front(tokens, gain, kv_gain, cos_t, sin_t, taps, ln_gain, ln_bias, weights):
     rows, width = tokens.shape
+    chans = taps.shape[1]
+    heads = weights[0].shape[1] // NOPE_DIM
+    rank = weights[2].shape[1]
     vmem = pl.BlockSpec(memory_space=pltpu.VMEM)
+    anywhere = pl.BlockSpec(memory_space=pl.ANY)
+    dma = pltpu.SemaphoreType.DMA
+    edge = 32
     return pl.pallas_call(
-        tokens_kernel,
+        front_kernel,
         out_shape=(
-            jax.ShapeDtypeStruct((rows, 2 * width), jnp.bfloat16),
-            jax.ShapeDtypeStruct((rows, 1), jnp.float32),
+            jax.ShapeDtypeStruct((heads, rows, 128), jnp.bfloat16),
+            jax.ShapeDtypeStruct((rank + ROT_DIM, rows), jnp.bfloat16),
+            jax.ShapeDtypeStruct((rows, chans), jnp.float32),
         ),
-        in_specs=[vmem] * 2,
-        out_specs=(vmem, vmem),
-        scratch_shapes=[
+        in_specs=[vmem] * 8 + [anywhere] * 6,
+        out_specs=(vmem,) * 3,
+        scratch_shapes=[pltpu.VMEM(weight.shape, jnp.bfloat16) for weight in weights]
+        + [
+            pltpu.VMEM((rows, 2 * width), jnp.bfloat16),
             pltpu.VMEM((rows, width), jnp.bfloat16),
-            pltpu.SemaphoreType.DMA,
-            pltpu.SemaphoreType.DMA,
-        ],
-        compiler_params=pltpu.CompilerParams(collective_id=0, has_side_effects=True),
-        name="token_exchange",
-    )(tokens, gain)
+            pltpu.VMEM((rows, 128), jnp.float32),
+            pltpu.VMEM((rows, chans), jnp.bfloat16),
+            pltpu.VMEM((edge, chans), jnp.bfloat16),
+            pltpu.VMEM((chans // 128, rows + edge, 128), jnp.float32),
+            pltpu.VMEM((rows, chans), jnp.float32),
+            pltpu.VMEM((rows, 256), jnp.float32),
+            pltpu.VMEM((rows, 256), jnp.float32),
+            dma((6,)),
+        ]
+        + [dma] * 6,
+        compiler_params=pltpu.CompilerParams(
+            vmem_limit_bytes=40 << 20, collective_id=0, has_side_effects=True
+        ),
+        name="front",
+    )(tokens, gain, kv_gain, cos_t, sin_t, taps, ln_gain, ln_bias, *weights)
 
 
 def output_kernel(
-    att_ref, swish_ref, att_gain, conv_gain, att_w, conv_w, out_ref,
-    sq_mine, sq_other, part, landed, sq_send, sq_recv, send, recv,
+    att_ref, swish_ref, att_gain, conv_gain, att_hbm, conv_hbm, out_ref,
+    att_w, conv_w, sq_mine, sq_other, part, landed, w_sem, sq_send, sq_recv, send, recv,
 ):
+    loads = [
+        pltpu.make_async_copy(att_hbm, att_w, w_sem.at[0]),
+        pltpu.make_async_copy(conv_hbm, conv_w, w_sem.at[1]),
+    ]
+    for load in loads:
+        load.start()
     mine = lax.axis_index("tp")
     rows, width = out_ref.shape
     lanes = sq_mine.shape[1] // 2
@@ -142,6 +289,8 @@
             + jnp.dot(conv_mixed, conv_w[:, cols], preferred_element_type=jnp.float32)
         ).astype(jnp.bfloat16)
 
+    for load in loads:
+        load.wait()
     copies = []
     for index in range(pieces):
         part[index] = product(1 - mine, index)
@@ -166,13 +315,16 @@
     return pl.pallas_call(
         output_kernel,
         out_shape=jax.ShapeDtypeStruct((rows, width), jnp.bfloat16),
-        in_specs=[vmem] * 6,
+        in_specs=[vmem] * 4 + [pl.BlockSpec(memory_space=pl.ANY)] * 2,
         out_specs=vmem,
         scratch_shapes=[
+            pltpu.VMEM(att_w.shape, jnp.bfloat16),
+            pltpu.VMEM(conv_w.shape, jnp.bfloat16),
             pltpu.VMEM((rows, 256), jnp.float32),
             pltpu.VMEM((rows, 256), jnp.float32),
             pltpu.VMEM((pieces, rows, width // pieces), jnp.bfloat16),
             pltpu.VMEM((pieces, rows, width // pieces), jnp.bfloat16),
+            pltpu.SemaphoreType.DMA((2,)),
             pltpu.SemaphoreType.DMA,
             pltpu.SemaphoreType.DMA,
             pltpu.SemaphoreType.DMA((pieces,)),
@@ -417,7 +569,7 @@
             dma((blocks,)),
         ],
         compiler_params=pltpu.CompilerParams(
-            vmem_limit_bytes=56 << 20, collective_id=2, has_side_effects=True
+            vmem_limit_bytes=24 << 20, collective_id=2, has_side_effects=True
         ),
         name="attention",
     )(q_heads, packed, key_up_t, value_up_t)
@@ -586,15 +738,32 @@
         conv_value_weight,
         conv_gate_weight,
     )
-    paired = lax.axis_size("tp") == 2 and lax.axis_size("sp") % PLANE == 0
-    if paired:
-        scaled, row_scale = exchange_tokens(tokens, input_gain[None, :])
-    else:
-        whole_rows = lax.all_gather(tokens, "tp", axis=1, tiled=True).astype(jnp.float32)
-        scaled = (whole_rows * input_gain[None, :]).astype(jnp.bfloat16)
-        row_scale = lax.rsqrt(
-            jnp.mean(whole_rows * whole_rows, axis=1, keepdims=True) + norm_eps
-        )
+    if lax.axis_size("tp") == 2 and lax.axis_size("sp") % PLANE == 0:
+        positions = lax.axis_index("sp") * tok_rows + jnp.arange(tok_rows, dtype=jnp.int32)
+        cos_table, sine_table = rotary_tables(positions, ROT_DIM // 2)
+        q_heads, packed, swished = front(
+            tokens,
+            input_gain[None, :],
+            kv_gain[None, :],
+            cos_table.T,
+            sine_table.T,
+            conv_taps,
+            conv_ln_gain[None, :],
+            conv_ln_bias[None, :],
+            weight_list,
+        )
+        attended = attention(q_heads, packed, key_up.T, value_up.T)
+        return merge(
+            attended,
+            swished,
+            att_out_gain[None, :],
+            conv_out_gain[None, :],
+            att_out_weight,
+            conv_out_weight,
+        )
+    whole_rows = lax.all_gather(tokens, "tp", axis=1, tiled=True).astype(jnp.float32)
+    scaled = (whole_rows * input_gain[None, :]).astype(jnp.bfloat16)
+    row_scale = lax.rsqrt(jnp.mean(whole_rows * whole_rows, axis=1, keepdims=True) + norm_eps)
 
     def add_product(weight):
         return jnp.dot(scaled, weight, preferred_element_type=jnp.float32)
@@ -634,16 +803,6 @@
     spread = moment_two / CONV_CH - mean_val * mean_val
     normed = (conv_out - mean_val[:, None]) * lax.rsqrt(spread + norm_eps)[:, None]
     swished = jax.nn.silu(normed * conv_ln_gain[None, :] + conv_ln_bias[None, :])
-    if paired:
-        attended = attention(q_heads, packed, key_up.T, value_up.T)
-        return merge(
-            attended,
-            swished,
-            att_out_gain[None, :],
-            conv_out_gain[None, :],
-            att_out_weight,
-            conv_out_weight,
-        )
     lat_all = lax.all_gather(packed, "sp", axis=0)
     attended = gathered_attention(q_heads, lat_all, key_up.T, value_up.T).astype(jnp.float32)
     att_sq, conv_sq = lax.psum(

time: 103 us -> 87.8 us (0.85)
  matrix products: 12 us -> 0 us
  other arithmetic: 7.89 us -> 0.18 us
  local copies, waits for them, and re-layouts: 10.3 us -> 17.1 us
  blocking collectives: 3.53 us -> 0 us
  Pallas kernels: 67.2 us -> 69.3 us
  starting transfers between devices: 1.28 us -> 0 us
    dot_general x6 -> x0, matrix products: 12 us -> none  [add_product(): return jnp.dot(scaled, weight, preferred_element_type=jnp.float32)]
    unnamed x31 -> x34, local copies, waits for them, and re-layouts: 8.01 us -> 17.1 us
    pallas_call x2 -> x1, Pallas kernels: 9.41 us -> 13.6 us  [front(): pl.pallas_call(front_kernel, out_shape=(jax.ShapeDtypeStruct((heads, rows...]
    psum x1 -> x0, blocking collectives: 3.53 us -> none  [shards(): lax.psum((jnp.sum(conv_out, axis=1), jnp.sum(conv_out * conv_out, axis=1)...]
    mul x1 -> x0, other arithmetic: 2.38 us -> none  [shards(): jax.nn.silu(normed * conv_ln_gain[None, :] + conv_ln_bias[None, :])]
    transpose x2 -> x0, other arithmetic: 1.65 us -> none  [the longest x1 1.65 us: shards(): jnp.transpose(jnp.concatenate([plain_q, turned_q, blank], axis=2).astype(...]
    reduce_sum x1 -> x0, other arithmetic: 1.31 us -> none  [shards(): jnp.sum(conv_out, axis=1)]
    ppermute x1 -> x0, starting transfers between devices: 1.28 us -> none  [shifted(): return lax.ppermute(block, axis, route)]
  transfers between devices with their start and end apart: 1 -> 0, of which waited for: 0 -> 0; matrix products, arithmetic and copies ran while one was open for 19% -> 0% of each run, Pallas kernels for 46% -> 0%
where the time goes in v3:
time: 87.8 us; the launch traced here: 86.6 us
  Pallas kernels  69.3 us (79%)
  local copies, waits for them, and re-layouts  17.1 us (19%)
    pallas_call x1, Pallas kernels, attention(): pl.pallas_call(attention_kernel, out_shape=jax.ShapeDtypeStruct((rows, va...  46.3 us
    unnamed x34, local copies, waits for them, and re-layouts  17.1 us
    pallas_call x1, Pallas kernels, front(): pl.pallas_call(front_kernel, out_shape=(jax.ShapeDtypeStruct((heads, rows...  13.6 us
    pallas_call x1, Pallas kernels, merge(): pl.pallas_call(output_kernel, out_shape=jax.ShapeDtypeStruct((rows, width...  9.29 us

profile of v3, /device:TPU:31, one launch (start us, length us, event | category | flops | bytes accessed | tf_op | source)
XLA Modules:
  0.0 86.6 jit_solution(5924735530049092113)
XLA Ops:
  0.0 0.2 multiply_sine_fusion
  0.2 1.2 %copy.19.rotw_hbm = bf16[2048,32]{1,0:T(8,128)(2,1)S(1)} copy(bf16[2048,32]{0,1:T(8,128)(2,1)} %param.23) | data formatting | bytes 262144 | tf_op args[5]
  1.4 0.0 copy-start
  1.4 1.6 %copy-done = bf16[2048,512]{1,0:T(8,128)(2,1)S(1)} copy-done((bf16[2048,512]{1,0:T(8,128)(2,1)S(1)}, bf16[2048,512]{1,0:T(8,128)(2,1)}, u32[]{:S(2)}) %copy-start) | copy-done | bytes 2097176
  3.0 0.0 copy-start.1
  3.0 1.6 %copy-done.1 = bf16[2048,512]{1,0:T(8,128)(2,1)S(1)} copy-done((bf16[2048,512]{1,0:T(8,128)(2,1)S(1)}, bf16[2048,512]{1,0:T(8,128)(2,1)}, u32[]{:S(2)}) %copy-start.1) | copy-done | bytes 2097176
  4.6 0.0 copy-start.2
  4.6 1.6 %copy-done.2 = bf16[2048,512]{1,0:T(8,128)(2,1)S(1)} copy-done((bf16[2048,512]{1,0:T(8,128)(2,1)S(1)}, bf16[2048,512]{1,0:T(8,128)(2,1)}, u32[]{:S(2)}) %copy-start.2) | copy-done | bytes 2097176
  6.2 0.0 copy-start.4
  6.2 1.2 %copy-done.4 = bf16[2048,256]{1,0:T(8,128)(2,1)S(1)} copy-done((bf16[2048,256]{1,0:T(8,128)(2,1)S(1)}, bf16[2048,256]{1,0:T(8,128)(2,1)}, u32[]{:S(2)}) %copy-start.4) | copy-done | bytes 1048600
  7.4 0.0 copy-start.5
  7.4 1.2 %copy-done.5 = bf16[2048,256]{1,0:T(8,128)(2,1)S(1)} copy-done((bf16[2048,256]{1,0:T(8,128)(2,1)S(1)}, bf16[2048,256]{1,0:T(8,128)(2,1)}, u32[]{:S(2)}) %copy-start.5) | copy-done | bytes 1048600
  8.6 0.0 copy-start.7
  8.6 1.1 %copy-done.7 = bf16[384,1024]{1,0:T(8,128)(2,1)S(1)} copy-done((bf16[384,1024]{1,0:T(8,128)(2,1)S(1)}, bf16[384,1024]{1,0:T(8,128)(2,1)}, u32[]{:S(2)}) %copy-start.7) | copy-done | bytes 786456
  9.7 0.0 copy-start.8
  9.7 0.8 copy-done.8
  10.6 0.0 copy-start.9
  10.6 0.7 copy-done.9
  11.3 0.0 copy-start.10
  11.3 0.7 copy-done.10
  12.0 0.0 copy-start.11
  12.0 0.7 copy-done.11
  12.6 0.0 copy-start.12
  12.6 0.7 copy-done.12
  13.3 0.0 copy-start.13
  13.3 0.0 copy-start.14
  13.3 13.6 %front.1 = (bf16[8,384,128]{2,1,0:T(8,128)(2,1)S(1)}, bf16[288,384]{1,0:T(8,128)(2,1)S(1)}, f32[384,512]{1,0:T(8,128)S(1)}) custom-call(bf16[384,1024]{1,0:T(8,128)(2,1)S(1)} %copy-done.7, f32[1,2048]{1,0:T(1,128)S(1)} %bitcast.10, f32[1,256]{1,0:T(1,128)S(1)} %bitcast.13, f32[16,384]{1,0:T(8,128)S(1)} %get-tuple-element.12.cos_ref, ...), custom_call_target="tpu_custom_call" | custom-call | tf_op jit(solution)/shard_map/front/pallas_call | solution.py:225
  27.0 0.0 copy-start.6
  27.0 0.9 %copy-done.6 = f32[384,512]{1,0:T(8,128)} copy-done((f32[384,512]{1,0:T(8,128)}, f32[384,512]{1,0:T(8,128)S(1)}, u32[]{:S(2)}) %copy-start.6) | copy-done | bytes 786456
  27.8 0.0 copy-done.13
  27.9 0.1 copy.20
  28.0 0.0 copy-done.14
  28.0 0.1 copy.21
  28.1 46.3 %attention.1.att_ref = bf16[384,512]{1,0:T(8,128)(2,1)S(1)} custom-call(bf16[8,384,128]{2,1,0:T(8,128)(2,1)S(1)} %get-tuple-element.8.q_ref, bf16[288,384]{1,0:T(8,128)(2,1)S(1)} %get-tuple-element.9.own_ref, bf16[512,256]{1,0:T(8,128)(2,1)S(1)} %bitcast.8, bf16[512,256]{1,0:T(8,128)(2,1)S(1)} %bitcast.9), custom_call_target="tpu_custom_call" | custom-call | tf_op jit(solution)/shard_map/attention/pallas_call | solution.py:554
  74.5 0.0 copy-start.3
  74.5 0.8 copy-done.3
  75.3 9.3 %output_merge.1 = bf16[384,1024]{1,0:T(8,128)(2,1)} custom-call(bf16[384,512]{1,0:T(8,128)(2,1)} %copy-done.3, f32[384,512]{1,0:T(8,128)} %copy-done.6, f32[1,512]{1,0:T(1,128)} %bitcast.14, f32[1,512]{1,0:T(1,128)} %bitcast.15, bf16[512,2048]{1,0:T(8,128)(2,1)} %att_hbm.1, bf16[512,2048]{1,0:T(8,128)(2,1)} %conv_hbm.1), custom_call_target="tpu_custom_call" | custom-call | tf_op jit(solution)/shard_map/output_merge/pallas_call | solution.py:315
  84.5 2.1 %copy.23 = bf16[384,1024]{1,0:T(8,128)(2,1)} copy(bf16[384,1024]{1,0:T(8,128)(2,1)} %output_merge.1) | data formatting | bytes 1572864
  (2 shorter events, 0.0 us)
Async XLA Ops:
  1.4 1.6 %copy-start = (bf16[2048,512]{1,0:T(8,128)(2,1)S(1)}, bf16[2048,512]{1,0:T(8,128)(2,1)}, u32[]{:S(2)}) copy-start(bf16[2048,512]{1,0:T(8,128)(2,1)} %qw_hbm.1) | copy-start | bytes 6291460
  3.0 1.6 %copy-start.1 = (bf16[2048,512]{1,0:T(8,128)(2,1)S(1)}, bf16[2048,512]{1,0:T(8,128)(2,1)}, u32[]{:S(2)}) copy-start(bf16[2048,512]{1,0:T(8,128)(2,1)} %cvw_hbm.1) | copy-start | bytes 6291460
  4.6 1.6 %copy-start.2 = (bf16[2048,512]{1,0:T(8,128)(2,1)S(1)}, bf16[2048,512]{1,0:T(8,128)(2,1)}, u32[]{:S(2)}) copy-start(bf16[2048,512]{1,0:T(8,128)(2,1)} %cgw_hbm.1) | copy-start | bytes 6291460
  6.2 1.2 %copy-start.4 = (bf16[2048,256]{1,0:T(8,128)(2,1)S(1)}, bf16[2048,256]{1,0:T(8,128)(2,1)}, u32[]{:S(2)}) copy-start(bf16[2048,256]{1,0:T(8,128)(2,1)} %qrw_hbm.1) | copy-start | bytes 3145732
  7.4 1.2 %copy-start.5 = (bf16[2048,256]{1,0:T(8,128)(2,1)S(1)}, bf16[2048,256]{1,0:T(8,128)(2,1)}, u32[]{:S(2)}) copy-start(bf16[2048,256]{1,0:T(8,128)(2,1)} %kvd_hbm.1) | copy-start | bytes 3145732
  8.6 1.1 %copy-start.7 = (bf16[384,1024]{1,0:T(8,128)(2,1)S(1)}, bf16[384,1024]{1,0:T(8,128)(2,1)}, u32[]{:S(2)}) copy-start(bf16[384,1024]{1,0:T(8,128)(2,1)} %tok_ref.1) | copy-start | bytes 2359300
  9.7 0.8 copy-start.8
  10.6 0.7 copy-start.9
  11.3 0.7 copy-start.10
  12.0 0.7 copy-start.11
  12.6 0.7 copy-start.12
  13.3 14.5 %copy-start.13 = (bf16[256,512]{1,0:T(8,128)(2,1)S(1)}, bf16[256,512]{1,0:T(8,128)(2,1)}, u32[]{:S(2)}) copy-start(bf16[256,512]{1,0:T(8,128)(2,1)} %param.25) | copy-start | bytes 786436
  13.3 14.7 %copy-start.14 = (bf16[256,512]{1,0:T(8,128)(2,1)S(1)}, bf16[256,512]{1,0:T(8,128)(2,1)}, u32[]{:S(2)}) copy-start(bf16[256,512]{1,0:T(8,128)(2,1)} %param.26) | copy-start | bytes 786436
  27.0 0.9 %copy-start.6 = (f32[384,512]{1,0:T(8,128)}, f32[384,512]{1,0:T(8,128)S(1)}, u32[]{:S(2)}) copy-start(f32[384,512]{1,0:T(8,128)S(1)} %get-tuple-element.10.swish_ref) | copy-start | bytes 2359300
  74.5 0.8 copy-start.3

commit v4 on v3

--- a/solution.py
+++ b/solution.py
@@ -146,9 +146,11 @@
             [front * cos_table - back * sin_table, back * cos_table + front * sin_table], axis=0
         )
 
-    narrow[...] = jnp.zeros(narrow.shape, jnp.float32)
-    narrow[:, : 2 * turn] = project(rotw) * row_scale
-    packed_ref[rank:, :] = rotate(narrow[...].T).astype(jnp.bfloat16)
+    narrow[...] = jnp.broadcast_to(row_scale, narrow.shape)
+    key_turn = lax.dot_general(
+        rotw[...], scaled[...], (((1,), (1,)), ((), ())), preferred_element_type=jnp.float32
+    )
+    packed_ref[rank:, :] = rotate(key_turn * narrow[...].T[: 2 * turn]).astype(jnp.bfloat16)
     loads[4].wait()
     loads[5].wait()
     query_scale = row_scale * (math.log2(math.e) / math.sqrt(NOPE_DIM + ROT_DIM))
@@ -219,7 +221,7 @@
     heads = weights[0].shape[1] // NOPE_DIM
     rank = weights[2].shape[1]
     vmem = pl.BlockSpec(memory_space=pltpu.VMEM)
-    anywhere = pl.BlockSpec(memory_space=pl.ANY)
+    anywhere = pl.BlockSpec(memory_space=pltpu.HBM)
     dma = pltpu.SemaphoreType.DMA
     edge = 32
     return pl.pallas_call(
@@ -246,7 +248,7 @@
         ]
         + [dma] * 6,
         compiler_params=pltpu.CompilerParams(
-            vmem_limit_bytes=40 << 20, collective_id=0, has_side_effects=True
+            vmem_limit_bytes=62 << 20, collective_id=0, has_side_effects=True
         ),
         name="front",
     )(tokens, gain, kv_gain, cos_t, sin_t, taps, ln_gain, ln_bias, *weights)
@@ -315,7 +317,7 @@
     return pl.pallas_call(
         output_kernel,
         out_shape=jax.ShapeDtypeStruct((rows, width), jnp.bfloat16),
-        in_specs=[vmem] * 4 + [pl.BlockSpec(memory_space=pl.ANY)] * 2,
+        in_specs=[vmem] * 4 + [pl.BlockSpec(memory_space=pltpu.HBM)] * 2,
         out_specs=vmem,
         scratch_shapes=[
             pltpu.VMEM(att_w.shape, jnp.bfloat16),
@@ -355,7 +357,6 @@
     layers = blocks // PLANE
     layer = me // PLANE
     spot = me % PLANE
-    last = me // pairing
     height = lat_ref.shape[1] // 2
     half = pl.ds(pl.multiple_of(core * height, 16), height)
 
@@ -452,10 +453,12 @@
             weights, vt[head], (((1,), (1,)), ((), ())), preferred_element_type=jnp.float32
         )
 
-    def visit(pair):
-        expand(pair)
+    def visit(group, middle):
+        expand(group)
         ahead = score(0)
         for head in range(heads):
+            if head == heads // 2:
+                middle()
             scores = ahead
             if head + 1 < heads:
                 ahead = score(head + 1)
@@ -470,48 +473,32 @@
     hand_over(0)
     relay(1)
     gathered(0)
-    expand(last)
-    key_pos = last * wide + lax.broadcasted_iota(jnp.int32, (rows, wide), 1)
+    expand(layer)
+    key_pos = layer * wide + lax.broadcasted_iota(jnp.int32, (rows, wide), 1)
     query_pos = me * rows + lax.broadcasted_iota(jnp.int32, (rows, wide), 0)
     hidden = key_pos > query_pos
     ahead = score(0)
     for head in range(heads):
+        if head == heads // 2:
+            hand_over(1)
+            relay(2)
         scores = jnp.where(hidden, far_below, ahead)
         if head + 1 < heads:
             ahead = score(head + 1)
         top = jnp.max(scores, axis=1, keepdims=True)
         run_max[head] = jnp.broadcast_to(top, (rows, lanes))
         acc[head] = weigh(head, scores, top)
-    hand_over(1)
-    relay(2)
-
-    per_layer = PLANE // pairing
-    first = layer * per_layer
-
-    def near(step, carry):
-        visit(last - 1 - step)
-        return carry
-
-    lax.fori_loop(0, last - first, near, 0)
 
     def far(step, carry):
-        gathered_all(step)
-
-        def one(turn, inner):
-            @pl.when(turn == 1)
-            def _():
-                hand_over(step + 1)
-                relay(step + 2)
-
-            visit((layer - step) * per_layer + per_layer - 1 - turn)
-            return inner
-
-        lax.fori_loop(0, per_layer, one, 0)
-        return carry
-
-    def gathered_all(step):
         for d in range(PLANE):
             core_copy((layer - step) * PLANE + spot_at(d)).wait_recv()
+
+        def middle():
+            hand_over(step + 1)
+            relay(step + 2)
+
+        visit(layer - step, middle)
+        return carry
 
     lax.fori_loop(1, layer + 1, far, 0)
     lane = lax.broadcasted_iota(jnp.int32, (rows, lanes), 1)
@@ -547,7 +534,7 @@
 def attention(q_heads, packed, key_up_t, value_up_t):
     heads, rows, lanes = q_heads.shape
     blocks = lax.axis_size("sp")
-    wide = 2 * rows
+    wide = PLANE * rows
     layers = blocks // PLANE
     vmem = pl.BlockSpec(memory_space=pltpu.VMEM)
     dma = pltpu.SemaphoreType.DMA
@@ -569,7 +556,7 @@
             dma((blocks,)),
         ],
         compiler_params=pltpu.CompilerParams(
-            vmem_limit_bytes=24 << 20, collective_id=2, has_side_effects=True
+            vmem_limit_bytes=40 << 20, collective_id=2, has_side_effects=True
         ),
         name="attention",
     )(q_heads, packed, key_up_t, value_up_t)
@@ -750,7 +737,7 @@
             conv_taps,
             conv_ln_gain[None, :],
             conv_ln_bias[None, :],
-            weight_list,
+            weight_list[:3] + (rot_down.T,) + weight_list[4:],
         )
         attended = attention(q_heads, packed, key_up.T, value_up.T)
         return merge(

time: 87.8 us -> 76.6 us (0.87)
  local copies, waits for them, and re-layouts: 17.1 us -> 7.03 us
  Pallas kernels: 69.3 us -> 68 us
    unnamed x34 -> x9, local copies, waits for them, and re-layouts: 17.1 us -> 7.03 us
    pallas_call x1, Pallas kernels: 46.3 us -> 43.3 us  [attention(): pl.pallas_call(attention_kernel, out_shape=jax.ShapeDtypeStruct((rows, va...]
    pallas_call x1, Pallas kernels: 13.6 us -> 15.4 us  [front(): pl.pallas_call(front_kernel, out_shape=(jax.ShapeDtypeStruct((heads, rows...]
where the time goes in v4:
time: 76.6 us; the launch traced here: 75.9 us
  Pallas kernels  68 us (89%)
  local copies, waits for them, and re-layouts  7.03 us (9%)
  other arithmetic  0.8 us (1%)
    pallas_call x1, Pallas kernels, attention(): pl.pallas_call(attention_kernel, out_shape=jax.ShapeDtypeStruct((rows, va...  43.3 us
    pallas_call x1, Pallas kernels, front(): pl.pallas_call(front_kernel, out_shape=(jax.ShapeDtypeStruct((heads, rows...  15.4 us
    pallas_call x1, Pallas kernels, merge(): pl.pallas_call(output_kernel, out_shape=jax.ShapeDtypeStruct((rows, width...  9.21 us
    unnamed x9, local copies, waits for them, and re-layouts  7.03 us

profile of v4, /device:TPU:31, one launch (start us, length us, event | category | flops | bytes accessed | tf_op | source)
XLA Modules:
  0.0 75.9 jit_solution(8317202703856731021)
XLA Ops:
  0.0 0.8 %multiply_sine_fusion = (f32[16,384]{1,0:T(8,128)}, f32[16,384]{1,0:T(8,128)}) fusion(f32[16]{0:T(128)S(1)} %multiply_power_fusion, f32[384]{0:T(512)S(1)} %add_convert_fusion), kind=kLoop, calls=%fused_computation | loop fusion | flops 6144 | bytes 50752 | tf_op jit(solution)/shard_map/sin | solution.py:33
  0.8 1.1 %copy.19 = bf16[256,512]{0,1:T(8,128)(2,1)S(1)} copy(bf16[256,512]{1,0:T(8,128)(2,1)} %param.25) | data formatting | bytes 524288 | tf_op args[7]
  1.9 1.1 %copy.20 = bf16[256,512]{0,1:T(8,128)(2,1)S(1)} copy(bf16[256,512]{1,0:T(8,128)(2,1)} %param.26) | data formatting | bytes 524288 | tf_op args[8]
  3.0 15.4 %front.1 = (bf16[8,384,128]{2,1,0:T(8,128)(2,1)}, bf16[288,384]{1,0:T(8,128)(2,1)}, f32[384,512]{1,0:T(8,128)}) custom-call(bf16[384,1024]{1,0:T(8,128)(2,1)} %tok_ref.1, f32[1,2048]{1,0:T(1,128)} %bitcast.12, f32[1,256]{1,0:T(1,128)} %bitcast.17, f32[16,384]{1,0:T(8,128)} %get-tuple-element.12.cos_ref, f32[16,384]{1,0:T(8,128)} %get-tuple-element.11.sin_ref, ...), custom_call_target="tpu_custom_call" | custom-call | tf_op jit(solution)/shard_map/front/pallas_call | solution.py:227
  18.4 0.0 copy-start.1
  18.4 1.1 %copy-done.1 = bf16[8,384,128]{2,1,0:T(8,128)(2,1)S(1)} copy-done((bf16[8,384,128]{2,1,0:T(8,128)(2,1)S(1)}, bf16[8,384,128]{2,1,0:T(8,128)(2,1)}, u32[]{:S(2)}) %copy-start.1) | copy-done | bytes 786456
  19.6 0.0 copy-start.2
  19.6 0.9 %copy-done.2 = bf16[288,384]{1,0:T(8,128)(2,1)S(1)} copy-done((bf16[288,384]{1,0:T(8,128)(2,1)S(1)}, bf16[288,384]{1,0:T(8,128)(2,1)}, u32[]{:S(2)}) %copy-start.2) | copy-done | bytes 221208
  20.5 43.3 %attention.1.att_ref = bf16[384,512]{1,0:T(8,128)(2,1)S(1)} custom-call(bf16[8,384,128]{2,1,0:T(8,128)(2,1)S(1)} %copy-done.1, bf16[288,384]{1,0:T(8,128)(2,1)S(1)} %copy-done.2, bf16[512,256]{1,0:T(8,128)(2,1)S(1)} %bitcast.9, bf16[512,256]{1,0:T(8,128)(2,1)S(1)} %bitcast.10), custom_call_target="tpu_custom_call" | custom-call | tf_op jit(solution)/shard_map/attention/pallas_call | solution.py:541
  63.8 0.0 copy-start
  63.8 0.7 copy-done
  64.6 9.2 %output_merge.1 = bf16[384,1024]{1,0:T(8,128)(2,1)} custom-call(bf16[384,512]{1,0:T(8,128)(2,1)} %copy-done, f32[384,512]{1,0:T(8,128)} %get-tuple-element.10.swish_ref, f32[1,512]{1,0:T(1,128)} %bitcast.13, f32[1,512]{1,0:T(1,128)} %bitcast.14, bf16[512,2048]{1,0:T(8,128)(2,1)} %att_hbm.1, bf16[512,2048]{1,0:T(8,128)(2,1)} %conv_hbm.1), custom_call_target="tpu_custom_call" | custom-call | tf_op jit(solution)/shard_map/output_merge/pallas_call | solution.py:317
  73.8 2.1 %copy.22 = bf16[384,1024]{1,0:T(8,128)(2,1)} copy(bf16[384,1024]{1,0:T(8,128)(2,1)} %output_merge.1) | data formatting | bytes 1572864
  (2 shorter events, 0.0 us)
Async XLA Ops:
  18.4 1.1 %copy-start.1 = (bf16[8,384,128]{2,1,0:T(8,128)(2,1)S(1)}, bf16[8,384,128]{2,1,0:T(8,128)(2,1)}, u32[]{:S(2)}) copy-start(bf16[8,384,128]{2,1,0:T(8,128)(2,1)} %get-tuple-element.8.q_ref) | copy-start | bytes 2359300
  19.6 0.9 %copy-start.2 = (bf16[288,384]{1,0:T(8,128)(2,1)S(1)}, bf16[288,384]{1,0:T(8,128)(2,1)}, u32[]{:S(2)}) copy-start(bf16[288,384]{1,0:T(8,128)(2,1)} %get-tuple-element.9.own_ref) | copy-start | bytes 663556
  63.8 0.7 copy-start
